TPU v7x, 256 devices: a whole 4x4x8 slice. The times are simulated.
256 devices in a mesh: sp: 32 (over z, x), tp: 8 (over y, core).
Axes of the slice: x: 4, y: 4, z: 8, core: 2. Of those that a mesh axis runs over, the one named last changes fastest.
Arguments:
- latents: bfloat16 [16384, 2048], P(('sp', 'tp')), may hold values from -6 to 6
- context: bfloat16 [512, 2048], P('sp'), may hold values from -6 to 6
- cond: float32 [2048], P('sp'), may hold values from -6 to 6
- ctx_cond: float32 [2048], P('sp'), may hold values from -6 to 6
- mod_weight: float32 [2048, 6144], P('sp', 'tp'), may hold values from -0.125 to 0.125
- query_weight: bfloat16 [2048, 2048], P(None, 'tp'), may hold values from -1 to 1, as said below
- key_matrix: bfloat16 [2048, 1024], P(None, 'tp'), may hold values from -1 to 1, as said below
- value_matrix: bfloat16 [2048, 1024], P(None, 'tp'), may hold values from -0.125 to 0.125
- out_weight: bfloat16 [2048, 2048], P('tp'), may hold values from -0.125 to 0.125
- query_gain: float32 [128], replicated, may hold values from 0.7 to 7
- key_gain: float32 [128], replicated, may hold values from 0.7 to 7
Outputs:
- updated: bfloat16 [16384, 2048], P(('sp', 'tp'))
Inputs may be any that keep to these rules, and one draw needn't show every extreme that they name: `query_weight`: entries of order 2048 to the power -1/2. `key_matrix`: entries of order 2048 to the power -1/2.
All inputs are finite; a program needn't handle non-finite values.
Results may differ from a plain program's by a relative error of at most 0.0085.
The roundings to bfloat16 on the way count: a program that leaves them out, or rounds other values in their place, can miss the bound.
Values may be sent and summed in bfloat16 or wider, within the bound.
A program may use at most 128 MiB of HBM per device.

v0:
```python
import math

import jax
import jax.numpy as jnp
from jax import lax
from jax.sharding import Mesh
from jax.sharding import PartitionSpec as P

GRID_W = 64
SP = ("sp_0", "sp_1")
SP_TP = ("sp_0", "sp_1", "tp")


NORM_EPS = 1e-06
ROPE_BASE = 10000.0


def over_axes(value, axes):
    for axis in axes:
        value = lax.psum(value, axis)
    return value


def side_by_side(arrays, axis, dim, along):
    both = jnp.concatenate(arrays, axis=along)
    filled, at, done = (lax.all_gather(both, axis, axis=dim, tiled=True), 0, [])
    for a in arrays:
        done.append(lax.slice_in_dim(filled, at, at + a.shape[along], axis=along))
        at += a.shape[along]
    return tuple(done)


def normalize(latent_value_rows):
    return latent_value_rows * lax.rsqrt(
        jnp.mean(latent_value_rows * latent_value_rows, axis=-1, keepdims=True) + NORM_EPS
    )


def rotate(latent_value_rows, positions):
    quarter = latent_value_rows.shape[-1] // 2
    inv_freq = ROPE_BASE ** (-jnp.arange(quarter, dtype=jnp.float32) / quarter)
    angles = positions.astype(jnp.float32)[:, None] * inv_freq[None, :]
    cos_table = jnp.cos(angles)[:, None, :]
    sin_table = jnp.sin(angles)[:, None, :]
    first, second = (latent_value_rows[..., :quarter], latent_value_rows[..., quarter:])
    return jnp.concatenate(
        [first * cos_table - second * sin_table, second * cos_table + first * sin_table], axis=-1
    )


def axial(latent_value_rows, positions):
    half_dim = latent_value_rows.shape[-1] // 2
    return jnp.concatenate(
        [
            rotate(latent_value_rows[..., :half_dim], positions // GRID_W),
            rotate(latent_value_rows[..., half_dim:], positions % GRID_W),
        ],
        axis=-1,
    )


def modulate(latent_value_rows, mod_row):
    model_width = latent_value_rows.shape[-1]
    shift_vec = mod_row[:model_width]
    scale_vec = mod_row[model_width : 2 * model_width]
    return (
        normalize(latent_value_rows.astype(jnp.float32)) * (1.0 + scale_vec) + shift_vec
    ).astype(jnp.bfloat16)


def body(
    latents,
    context,
    cond,
    ctx_cond,
    mod_weight,
    query_weight,
    key_matrix,
    value_matrix,
    out_weight,
    query_gain,
    key_gain,
):
    model_width = latents.shape[1]
    head_dim = query_gain.shape[0]
    sp_count = lax.axis_size(SP)
    partials = jnp.dot(
        jax.nn.silu(jnp.stack([cond, ctx_cond])), mod_weight, precision=lax.Precision.HIGHEST
    )
    summed = over_axes(partials, SP)
    modulation = lax.all_gather(summed, "tp", axis=1, tiled=True)
    gate_vec = modulation[0, 2 * model_width :]
    normalised_rows = modulate(latents, modulation[0])
    prefix_normalised = modulate(context, modulation[1])
    query_cols = query_weight.shape[1]
    key_cols = key_matrix.shape[1]
    piece = lax.all_gather(normalised_rows, "tp", axis=0, tiled=True)
    projected = jnp.concatenate(
        [
            jnp.dot(piece, query_weight, preferred_element_type=jnp.float32),
            jnp.dot(piece, key_matrix, preferred_element_type=jnp.float32),
            jnp.dot(piece, value_matrix, preferred_element_type=jnp.float32),
        ],
        axis=1,
    )
    row_count = projected.shape[0]
    positions = lax.axis_index(SP) * row_count + jnp.arange(row_count, dtype=jnp.int32)
    query_heads = projected[:, :query_cols].reshape(row_count, -1, head_dim)
    query_heads = axial(normalize(query_heads) * query_gain, positions).astype(jnp.bfloat16)
    key_heads = projected[:, query_cols : query_cols + key_cols].reshape(row_count, -1, head_dim)
    key_heads = axial(normalize(key_heads) * key_gain, positions).astype(jnp.bfloat16)
    value_heads = (
        projected[:, query_cols + key_cols :].reshape(row_count, -1, head_dim).astype(jnp.bfloat16)
    )
    key_part = jnp.dot(prefix_normalised, key_matrix, preferred_element_type=jnp.float32).reshape(
        prefix_normalised.shape[0], -1, head_dim
    )
    value_part = jnp.dot(
        prefix_normalised, value_matrix, preferred_element_type=jnp.float32
    ).reshape(prefix_normalised.shape[0], -1, head_dim)
    local_keys = (normalize(key_part) * key_gain).astype(jnp.bfloat16)
    local_values = value_part.astype(jnp.bfloat16)
    prefix_keys, prefix_values = side_by_side((local_keys, local_values), SP, 0, 1)
    kv_local = key_heads.shape[1]
    group_size = query_heads.shape[1] // kv_local
    grouped = query_heads.reshape(row_count, kv_local, group_size, head_dim).transpose(1, 2, 0, 3)
    grouped = grouped.reshape(kv_local, group_size * row_count, head_dim)
    inv_root = head_dim ** (-0.5)
    lift = math.log(sp_count * row_count / (2.0 * prefix_keys.shape[0]))
    ctx_scores = (
        jnp.einsum("hqd,khd->hqk", grouped, prefix_keys, preferred_element_type=jnp.float32)
        * inv_root
        + lift
    )
    top_init = jnp.max(ctx_scores, axis=-1)
    ctx_weights = jnp.exp(ctx_scores - top_init[..., None])
    initial = (
        top_init,
        jnp.sum(ctx_weights, axis=-1),
        jnp.einsum(
            "hqk,khd->hqd",
            ctx_weights.astype(jnp.bfloat16),
            prefix_values,
            preferred_element_type=jnp.float32,
        ),
    )

    def update(state_now, key_block, value_block):
        top_old, total_old, acc_old = state_now
        scores = (
            jnp.einsum("hqd,khd->hqk", grouped, key_block, preferred_element_type=jnp.float32)
            * inv_root
        )
        top_new = jnp.maximum(top_old, jnp.max(scores, axis=-1))
        factor = jnp.exp(top_old - top_new)
        weights_now = jnp.exp(scores - top_new[..., None])
        acc_new = acc_old * factor[..., None] + jnp.einsum(
            "hqk,khd->hqd",
            weights_now.astype(jnp.bfloat16),
            value_block,
            preferred_element_type=jnp.float32,
        )
        return (top_new, total_old * factor + jnp.sum(weights_now, axis=-1), acc_new)

    key_piece, value_piece = side_by_side((key_heads, value_heads), SP, 0, 1)
    key_count = key_piece.shape[0]
    rows_per_block = math.gcd(key_count, 2048)
    block_count = key_count // rows_per_block
    key_blocks = key_piece.reshape(block_count, rows_per_block, kv_local, head_dim)
    value_blocks = value_piece.reshape(block_count, rows_per_block, kv_local, head_dim)

    def one_step(state_in, blocks_in):
        return (update(state_in, blocks_in[0], blocks_in[1]), None)

    state_out, _ = lax.scan(one_step, initial, (key_blocks, value_blocks))
    top_fin, total_fin, acc_fin = state_out
    attended = (acc_fin / total_fin[..., None]).astype(jnp.bfloat16)
    attended = (
        attended.reshape(kv_local, group_size, row_count, head_dim)
        .transpose(2, 0, 1, 3)
        .reshape(row_count, -1)
    )
    exchanged = lax.all_to_all(attended, "tp", split_axis=0, concat_axis=1, tiled=True)
    mixed_rows = jnp.dot(
        exchanged,
        lax.all_gather(out_weight, "tp", axis=0, tiled=True),
        preferred_element_type=jnp.float32,
    )
    return (latents.astype(jnp.float32) + gate_vec * normalize(mixed_rows)).astype(jnp.bfloat16)


def solution(mesh):
    torus = Mesh(mesh.devices.reshape(8, 4, mesh.shape["tp"]), ("sp_0", "sp_1", "tp"))
    placed = (
        P(SP_TP, None),
        P(SP, None),
        P(SP),
        P(SP),
        P(SP, "tp"),
        P(None, "tp"),
        P(None, "tp"),
        P(None, "tp"),
        P("tp", None),
        P(),
        P(),
    )
    return jax.shard_map(
        body, mesh=torus, in_specs=placed, out_specs=P(SP_TP, None), check_vma=False
    )
```

profile of v0, /device:TPU:1, one launch (start us, length us, event | category | flops | bytes accessed | tf_op | source)
XLA Modules:
  0.0 285.0 jit_solution(6609689054624795851)
XLA Ops:
  6.5 1.3 fusion.67
  7.8 17.5 %psum.14 = f32[2,768]{1,0:T(2,128)S(1)} all-reduce(f32[2,768]{1,0:T(2,128)S(1)} %fusion.67), channel_id=1, replica_groups=mesh['sp_0'=8,'sp_1'=4,'tp'=8] {'sp_0'}, use_global_device_ids=true, to_apply=%region_0.1 | all-reduce | flops 1536 | bytes 12288 | tf_op jit(solution)/shard_map/psum | solution.py:20
  25.3 8.6 %psum.15 = f32[2,768]{1,0:T(2,128)S(1)} all-reduce(f32[2,768]{1,0:T(2,128)S(1)} %psum.14), channel_id=1, replica_groups=mesh['sp_0'=8,'sp_1'=4,'tp'=8] {'sp_1'}, use_global_device_ids=true, to_apply=%region_1.2 | all-reduce | flops 1536 | bytes 12288 | tf_op jit(solution)/shard_map/psum | solution.py:20
  33.9 19.5 %all_gather.15 = f32[2,6144]{1,0:T(2,128)S(1)} all-gather(f32[2,768]{1,0:T(2,128)S(1)} %psum.15), channel_id=1, replica_groups=mesh['sp_0'=8,'sp_1'=4,'tp'=8] {'tp'}, dimensions={1}, use_global_device_ids=true | all-gather | bytes 55296 | tf_op jit(solution)/shard_map/all_gather | solution.py:91
  53.4 1.1 fusion.28
  54.5 1.8 fusion.31
  56.5 23.1 %all-gather.4.cloned.1.call-done = bf16[512,2048]{1,0:T(8,128)(2,1)} async-done(((bf16[64,2048]{1,0:T(8,128)(2,1)}), bf16[512,2048]{1,0:T(8,128)(2,1)}) %all-gather.4.cloned.1.call-update) | async-done | bytes 2097168 | tf_op jit(solution)/shard_map/all_gather | solution.py:97
  79.5 2.5 multiply_reduce_fusion.3
  82.7 2.5 fusion.22
  86.8 3.0 %multiply_cosine_fusion.1 = (f32[512,32]{1,0:T(8,128)S(1)}, f32[512,32]{1,0:T(8,128)}, f32[512,32]{1,0:T(8,128)}, f32[512,32]{1,0:T(8,128)}) fusion(f32[32]{0:T(128)S(1)} %multiply_power_fusion, f32[512]{0:T(512)S(1)} %get-tuple-element.112, f32[512]{0:T(512)S(1)} %get-tuple-element.113), kind=kLoop, calls=%fused_computation.50 | loop fusion | flops 32768 | bytes 266368 | tf_op jit(solution)/shard_map/cos | solution.py:43
  89.9 1.3 fusion.23
  91.2 1.4 multiply_reduce_fusion.4
  92.6 40.4 %all_gather.17 = bf16[512,2,128]{2,0,1:T(8,128)(2,1)} all-gather(bf16[16,2,128]{2,0,1:T(8,128)(2,1)S(1)} %pad_maximum_fusion.2), channel_id=1, replica_groups=mesh['sp_0'=8,'sp_1'=4,'tp'=8] {'sp_0','sp_1'}, dimensions={0}, use_global_device_ids=true | all-gather | bytes 270336 | tf_op jit(solution)/shard_map/all_gather | solution.py:26
  133.1 1.6 multiply_reduce_fusion.2
  134.7 1.3 copy.16
  136.2 1.6 fusion.33
  139.6 46.4 %all-gather.6.cloned.1.call-done = bf16[16384,2,128]{0,2,1:T(8,128)(2,1)} async-done(((bf16[512,2,128]{0,2,1:T(8,128)(2,1)}), bf16[16384,2,128]{0,2,1:T(8,128)(2,1)}) %all-gather.6.cloned.1.call-update) | async-done | bytes 8388624 | tf_op jit(solution)/shard_map/all_gather | solution.py:26
  186.1 5.8 %fusion.76 = (bf16[16384,1,128]{0,2,1:T(8,128)(2,1)}, bf16[16384,1,128]{0,2,1:T(8,128)(2,1)}) fusion(bf16[16384,2,128]{0,2,1:T(8,128)(2,1)} %all-gather.6.cloned.1.call-done), kind=kLoop, calls=%fused_computation.126 | loop fusion | bytes 16777216 | tf_op jit(solution)/shard_map/slice | solution.py:28
  191.9 6.3 %copy.23 = bf16[16384,1,128]{2,0,1:T(8,128)(2,1)} copy(bf16[16384,1,128]{0,2,1:T(8,128)(2,1)} %get-tuple-element.78) | data formatting | bytes 8388608 | tf_op jit(solution)/shard_map/while | solution.py:175
  198.2 6.5 %copy.24 = bf16[16384,1,128]{2,0,1:T(8,128)(2,1)} copy(bf16[16384,1,128]{0,2,1:T(8,128)(2,1)} %get-tuple-element.77) | data formatting | bytes 8388608 | tf_op jit(solution)/shard_map/while | solution.py:175
  204.7 52.6 %while.14 = (s32[]{:T(128)}, f32[1,1024]{1,0:T(1,128)S(1)}, f32[1,1024]{1,0:T(1,128)S(1)}, f32[1,1024,128]{2,1,0:T(8,128)S(1)}, bf16[8,2048,1,128]{3,1,2,0:T(8,1...) while((s32[]{:T(128)}, f32[1,1024]{1,0:T(1,128)S(1)}, ...), condition=%wide.region_12.13_spmd, body=%wide.region_9.12_spmd.sunk | while | flops 1090783232 | bytes 27590756 | solution.py:175
  204.7 2.3 multiply_reduce_fusion.6
  207.0 1.4 fusion.96
  208.5 2.8 fusion.97
  211.3 2.3 multiply_reduce_fusion.6
  213.6 1.4 fusion.96
  215.1 2.8 fusion.97
  217.9 2.3 multiply_reduce_fusion.6
  220.2 1.4 fusion.96
  221.6 2.8 fusion.97
  224.4 2.3 multiply_reduce_fusion.6
  226.8 1.4 fusion.96
  228.2 2.8 fusion.97
  231.0 2.3 multiply_reduce_fusion.6
  233.3 1.4 fusion.96
  234.8 2.8 fusion.97
  237.6 2.3 multiply_reduce_fusion.6
  239.9 1.4 fusion.96
  241.4 2.8 fusion.97
  244.2 2.3 multiply_reduce_fusion.6
  246.5 1.4 fusion.96
  247.9 2.8 fusion.97
  250.7 2.3 multiply_reduce_fusion.6
  253.0 1.4 fusion.96
  254.5 2.8 fusion.97
  258.0 14.5 %all_to_all.19 = bf16[8,64,256]{2,1,0:T(8,128)(2,1)S(1)} all-to-all(bf16[8,64,256]{2,1,0:T(8,128)(2,1)S(1)} %all_to_all.14), channel_id=1, replica_groups=mesh['sp_0'=8,'sp_1'=4,'tp'=8] {'tp'}, dimensions={0} | all-to-all | bytes 524288 | tf_op jit(solution)/shard_map/all_to_all | solution.py:183
  272.5 5.1 %multiply_reduce_fusion.1 = (f32[64]{0:T(128)S(1)}, f32[64,2048]{1,0:T(8,128)S(1)}) fusion(bf16[64,2048]{1,0:T(8,128)(2,1)S(1)} %bitcast.110, bf16[2048,2048]{1,0:T(8,128)(2,1)} %all-gather.8.cloned.1.call-done), kind=kOutput, calls=%fused_computation.39 | convolution fusion | flops 537132992 | bytes 9175296 | tf_op jit(solution)/shard_map/dot_general | solution.py:184
  277.6 0.9 fusion.32
  (69 shorter events, 5.5 us)
Async XLA Ops:
  6.5 126.6 %copy-start = (bf16[2048,256]{1,0:T(8,128)(2,1)S(1)}, bf16[2048,256]{1,0:T(8,128)(2,1)}, u32[]{:S(2)}) copy-start(bf16[2048,256]{1,0:T(8,128)(2,1)} %param.18) | copy-start | bytes 3145732
  6.5 75.5 %copy-start.5 = (f32[128]{0:T(128)S(1)}, f32[128]{0:T(128)}, u32[]{:S(2)}) copy-start(f32[128]{0:T(128)} %param.23) | copy-start | bytes 1540
  6.5 73.0 %all-gather.4.cloned.1.call-start = ((), (), s32[]{:S(2)}) async-start(), calls=%async_computation.1 | async-start | bytes 2359296 | tf_op jit(solution)/shard_map/all_gather | solution.py:97
  56.4 129.7 %all-gather.6.cloned.1.call-start = ((), (), s32[]{:S(2)}) async-start(), calls=%async_computation.2 | async-start | bytes 8650752 | tf_op jit(solution)/shard_map/all_gather | solution.py:26
  56.4 33.3 %copy-start.4 = (bf16[16,2048]{1,0:T(8,128)(2,1)S(1)}, bf16[16,2048]{1,0:T(8,128)(2,1)}, u32[]{:S(2)}) copy-start(bf16[16,2048]{1,0:T(8,128)(2,1)} %param.14) | copy-start | bytes 196612
  82.1 51.0 %copy-start.1 = (bf16[512,2048]{1,0:T(8,128)(2,1)S(1)}, bf16[512,2048]{1,0:T(8,128)(2,1)}, u32[]{:S(2)}) copy-start(bf16[512,2048]{1,0:T(8,128)(2,1)} %all-gather.4.cloned.1.call-done) | copy-start | bytes 6291460
  86.0 49.9 %copy-start.6 = (f32[128]{0:T(128)S(1)}, f32[128]{0:T(128)}, u32[]{:S(2)}) copy-start(f32[128]{0:T(128)} %param.22) | copy-start | bytes 1540
  86.0 186.5 %all-gather.8.cloned.1.call-start = ((), (), s32[]{:S(2)}) async-start(), calls=%async_computation.3 | async-start | bytes 9437184 | tf_op jit(solution)/shard_map/all_gather | solution.py:186
  134.7 3.5 %copy-start.3 = (bf16[512,2,128]{2,0,1:T(8,128)(2,1)S(1)}, bf16[512,2,128]{2,0,1:T(8,128)(2,1)}, u32[]{:S(2)}) copy-start(bf16[512,2,128]{2,0,1:T(8,128)(2,1)} %all_gather.17) | copy-start | bytes 786436
  272.5 5.1 %copy-start.2 = (bf16[64,2048]{1,0:T(8,128)(2,1)S(1)}, bf16[64,2048]{1,0:T(8,128)(2,1)}, u32[]{:S(2)}) copy-start(bf16[64,2048]{1,0:T(8,128)(2,1)} %param.13) | copy-start | bytes 786436
Sparse Core Ops, SparseCore 0:
  56.5 23.0 all-gather.3
  86.1 99.8 all-gather.5
  187.9 54.6 all-gather.7
where the time goes:
time: 286 us; the launch traced here: 285 us
  blocking collectives  100 us (35%)
  waiting for transfers between devices  70.3 us (25%)
  matrix products  57.2 us (20%)
  other arithmetic  22.9 us (8%)
  local copies, waits for them, and re-layouts  20.4 us (7%)
  between operations  13.4 us (5%)
    all_gather x1, waiting for transfers between devices, side_by_side(): filled, at, done = (lax.all_gather(both, axis, axis=dim, tiled=True), 0, [])  46.4 us
    all_gather x1, blocking collectives, side_by_side(): filled, at, done = (lax.all_gather(both, axis, axis=dim, tiled=True), 0, [])  40.4 us
    psum x2, blocking collectives, over_axes(): value = lax.psum(value, axis)  26.1 us
    all_gather x1, waiting for transfers between devices, body(): piece = lax.all_gather(normalised_rows, 'tp', axis=0, tiled=True)  23.1 us
    dot_general x8, matrix products, update(): jnp.einsum('hqk,khd->hqd', weights_now.astype(jnp.bfloat16), value_block,...  22.2 us
    all_gather x1, blocking collectives, body(): modulation = lax.all_gather(summed, 'tp', axis=1, tiled=True)  19.5 us
    dot_general x8, matrix products, update(): jnp.einsum('hqd,khd->hqk', grouped, key_block, preferred_element_type=jnp...  18.4 us
    all_to_all x1, blocking collectives, body(): lax.all_to_all(attended, 'tp', split_axis=0, concat_axis=1, tiled=True)  14.5 us
  transfers between devices with their start and end apart: 3, of which 2 were waited for; matrix products, arithmetic and copies ran while one was open for 29% of the time, Pallas kernels for 0%

commit v1 on v0

v1 whole, which is shorter than its diff:
```python
import functools
import math

import jax
import jax.numpy as jnp
import numpy as np
from jax import lax
from jax.experimental import pallas as pl
from jax.experimental.pallas import tpu as pltpu
from jax.sharding import Mesh
from jax.sharding import PartitionSpec as P

GRID_W = 64
NORM_EPS = 1e-06
ROPE_BASE = 10000.0
Z, X, Y, C = 8, 4, 4, 2
AXES = ("z", "x", "y", "c")
SP = ("z", "x")
TP = ("y", "c")
MESH = pl.DeviceIdType.MESH
D = 2048
HEAD = 128
ROWS = 64
CTX_ROWS = 16
GROUP_ROWS = ROWS * Y * C
UNIT = CTX_ROWS + GROUP_ROWS
TOTAL_KEYS = UNIT * Z * X
LIFT = 16.0
SCORE_SCALE = HEAD ** (-0.5) * math.log2(math.e)


def coords():
    return tuple(lax.axis_index(a) for a in AXES)


def remote(src, dst, send, recv, dev):
    return pltpu.make_async_remote_copy(
        src_ref=src, dst_ref=dst, send_sem=send, recv_sem=recv, device_id=dev, device_id_type=MESH
    )


def meet(peers):
    barrier = pltpu.get_barrier_semaphore()
    for dev in peers:
        pl.semaphore_signal(barrier, inc=1, device_id=dev, device_id_type=MESH)
    pl.semaphore_wait(barrier, len(peers))


def rope_tables():
    quarter = HEAD // 4
    freq = (np.float32(ROPE_BASE) ** (-np.arange(quarter, dtype=np.float32) / np.float32(quarter))).astype(np.float32)
    lanes = freq[np.arange(HEAD) % quarter]
    sign = np.where(np.arange(HEAD) % (HEAD // 2) < quarter, -1.0, 1.0)
    grid_rows = GROUP_ROWS * Z * X // GRID_W
    row_angle = (np.arange(grid_rows, dtype=np.float32)[:, None] * lanes[None]).astype(np.float64)
    col_angle = (np.arange(GRID_W, dtype=np.float32)[:, None] * lanes[None]).astype(np.float64)
    as32 = lambda a: jnp.asarray(a.astype(np.float32))
    return (
        as32(np.cos(row_angle)),
        as32(np.sin(row_angle) * sign),
        as32(np.cos(col_angle)),
        as32(np.sin(col_angle) * sign),
    )


def column(row):
    n = row.shape[1]
    eye = lax.broadcasted_iota(jnp.int32, (n, n), 0) == lax.broadcasted_iota(jnp.int32, (n, n), 1)
    return jnp.sum(jnp.where(eye, row, 0.0), axis=1, keepdims=True)


def front_kernel(
    lat, ctx, cond, ctx_cond, modw, wq, wk, wv, q_gain, k_gain, cos_r, sin_r, cos_c, sin_c,
    q_out, kv_out, gate_out,
    xg, ws, cr, sr, part, x_in, x_sum, z_in, mod, xn, proj,
    w_sem, lat_send, lat_recv, x_send, x_recv, z_send, z_recv, t_send, t_recv,
):
    z, x, y, c = coords()
    me = y * C + c
    sp = z * X + x
    up, down = lax.rem(y + 1, Y), lax.rem(y + Y - 1, Y)
    far = lax.rem(y + 2, Y)
    loads = [
        pltpu.make_async_copy(wq, ws.at[:, pl.ds(0, 2 * HEAD)], w_sem.at[0]),
        pltpu.make_async_copy(wk, ws.at[:, pl.ds(2 * HEAD, HEAD)], w_sem.at[1]),
        pltpu.make_async_copy(wv, ws.at[:, pl.ds(3 * HEAD, HEAD)], w_sem.at[2]),
        pltpu.make_async_copy(cos_r.at[pl.ds(sp * 8, 8)], cr, w_sem.at[3]),
        pltpu.make_async_copy(sin_r.at[pl.ds(sp * 8, 8)], sr, w_sem.at[4]),
    ]
    for copy in loads:
        copy.start()
    x_peers = [(z, lax.rem(x + r, X), y, c) for r in range(1, X)]
    z_peers = [(lax.rem(z + r, Z), x, y, c) for r in range(1, Z)]
    t_rel = [(ry, rc) for ry in range(Y) for rc in range(C) if (ry, rc) != (0, 0)]
    t_peers = [(z, x, lax.rem(y + ry, Y), c + rc * (1 - 2 * c)) for ry, rc in t_rel]
    sib = (z, x, y, 1 - c)
    meet(x_peers + z_peers + t_peers)

    def slot(yy, cc):
        return yy * C + cc

    sends = []

    def send_lat(i, src, yy, cc, dev, lo=0, n=ROWS):
        copy = remote(src, xg.at[slot(yy, cc), pl.ds(lo, n)], lat_send.at[i], lat_recv.at[i], dev)
        copy.start()
        sends.append(copy)
        return copy

    up_dev, down_dev = (z, x, up, c), (z, x, down, c)
    c0 = send_lat(0, lat, y, c, up_dev)
    c1 = send_lat(1, lat, y, c, down_dev)
    c2 = send_lat(2, lat, y, c, sib)

    w = modw[...]
    for r, vec in enumerate((cond, ctx_cond)):
        v = vec[...]
        v = column(v * lax.logistic(v))
        row = jnp.sum(v * w, axis=0, keepdims=True)
        for i in range(6):
            part[r * 6 + i : r * 6 + i + 1, :] = row[:, i * HEAD : (i + 1) * HEAD]
    part[12:16, :] = jnp.zeros((4, HEAD), jnp.float32)
    xg[me] = lat[...]

    xs = [remote(part, x_in.at[i], x_send.at[i], x_recv.at[i], d) for i, d in enumerate(x_peers)]
    for s in xs:
        s.start()
    for s in xs:
        s.wait_recv()
    x_sum[...] = part[...] + x_in[0] + x_in[1] + x_in[2]
    zs = [remote(x_sum, z_in.at[i], z_send.at[i], z_recv.at[i], d) for i, d in enumerate(z_peers)]
    for s in zs:
        s.start()

    half = ROWS // 2
    c0.wait_recv()
    c3 = send_lat(3, xg.at[slot(down, c), pl.ds(0, half)], down, c, up_dev, 0, half)
    c5 = send_lat(5, xg.at[slot(down, c)], down, c, sib)
    c1.wait_recv()
    c4 = send_lat(4, xg.at[slot(up, c), pl.ds(half, half)], up, c, down_dev, half, half)
    c6 = send_lat(6, xg.at[slot(up, c)], up, c, sib)

    for s in zs:
        s.wait_recv()
    total = x_sum[...]
    for i in range(Z - 1):
        total = total + z_in[i]
    mod[me] = total
    ts = [remote(mod.at[me], mod.at[me], t_send.at[i], t_recv.at[i], d) for i, d in enumerate(t_peers)]
    for s in ts:
        s.start()
    c3.wait_recv()
    c4.wait_recv()
    c7 = send_lat(7, xg.at[slot(far, c)], far, c, sib)
    for copy in loads:
        copy.wait()
    for s in ts:
        s.wait_recv()

    def mod_row(r, first):
        tiles = [first + t for t in range(D // HEAD)]
        return jnp.concatenate([mod[t // 6, r * 6 + t % 6 : r * 6 + t % 6 + 1, :] for t in tiles], axis=1)

    gate_out[...] = mod_row(0, 32)

    def modulated(rows, r):
        v = rows.astype(jnp.float32)
        v = v * lax.rsqrt(jnp.mean(v * v, axis=-1, keepdims=True) + NORM_EPS)
        return (v * (1.0 + mod_row(r, 16)) + mod_row(r, 0)).astype(jnp.bfloat16)

    xn[:CTX_ROWS, :] = modulated(ctx[...], 1)
    for s in (c2, c5, c6, c7):
        s.wait_recv()
    for j in range(Y * C):
        xn[CTX_ROWS + ROWS * j : CTX_ROWS + ROWS * (j + 1), :] = modulated(xg[j], 0)

    lane = lax.broadcasted_iota(jnp.int32, (GRID_W, HEAD), 1)
    is_row = lane < HEAD // 2
    is_first = lax.rem(lane, HEAD // 2) < HEAD // 4

    def unit_rows(v, gain):
        return v * lax.rsqrt(jnp.mean(v * v, axis=-1, keepdims=True) + NORM_EPS) * gain

    for lo, n in ((0, UNIT // 2 + 8), (UNIT // 2 + 8, UNIT // 2 - 8)):
        proj[lo : lo + n, :] = jnp.dot(xn[lo : lo + n, :], ws[...], preferred_element_type=jnp.float32)
    qg, kg = q_gain[...], k_gain[...]
    kv_out[:CTX_ROWS, :HEAD] = unit_rows(proj[:CTX_ROWS, 2 * HEAD : 3 * HEAD], kg).astype(jnp.bfloat16)
    kv_out[:CTX_ROWS, HEAD:] = proj[:CTX_ROWS, 3 * HEAD :].astype(jnp.bfloat16) * jnp.bfloat16(LIFT)
    for j in range(GROUP_ROWS // GRID_W):
        lo = CTX_ROWS + GRID_W * j
        cos = jnp.where(is_row, cr[j : j + 1, :], cos_c[...])
        sin = jnp.where(is_row, sr[j : j + 1, :], sin_c[...])

        def turned(v, gain):
            v = unit_rows(v, gain)
            other = jnp.where(is_first, pltpu.roll(v, HEAD - HEAD // 4, 1), pltpu.roll(v, HEAD // 4, 1))
            return (v * cos + other * sin).astype(jnp.bfloat16)

        for h in range(2):
            q_out[GRID_W * j : GRID_W * (j + 1), h * HEAD : (h + 1) * HEAD] = turned(
                proj[lo : lo + GRID_W, h * HEAD : (h + 1) * HEAD], qg
            )
        kv_out[lo : lo + GRID_W, :HEAD] = turned(proj[lo : lo + GRID_W, 2 * HEAD : 3 * HEAD], kg)
        kv_out[lo : lo + GRID_W, HEAD:] = proj[lo : lo + GRID_W, 3 * HEAD :].astype(jnp.bfloat16)

    for s in sends + xs + zs + ts:
        s.wait_send()


def front(latents, context, cond, ctx_cond, mod_weight, wq, wk, wv, q_gain, k_gain):
    vm = pl.BlockSpec(memory_space=pltpu.VMEM)
    hbm = pl.BlockSpec(memory_space=pl.ANY)
    cos_r, sin_r, cos_c, sin_c = rope_tables()
    bf, f32 = jnp.bfloat16, jnp.float32
    dma = pltpu.SemaphoreType.DMA
    return pl.pallas_call(
        front_kernel,
        name="front",
        out_shape=(
            jax.ShapeDtypeStruct((GROUP_ROWS, 2 * HEAD), bf),
            jax.ShapeDtypeStruct((UNIT, 2 * HEAD), bf),
            jax.ShapeDtypeStruct((1, D), f32),
        ),
        in_specs=[vm] * 5 + [hbm] * 3 + [vm] * 2 + [hbm] * 2 + [vm] * 2,
        out_specs=(vm, vm, vm),
        scratch_shapes=[
            pltpu.VMEM((Y * C, ROWS, D), bf),
            pltpu.VMEM((D, 4 * HEAD), bf),
            pltpu.VMEM((8, HEAD), f32),
            pltpu.VMEM((8, HEAD), f32),
            pltpu.VMEM((16, HEAD), f32),
            pltpu.VMEM((X - 1, 16, HEAD), f32),
            pltpu.VMEM((16, HEAD), f32),
            pltpu.VMEM((Z - 1, 16, HEAD), f32),
            pltpu.VMEM((Y * C, 16, HEAD), f32),
            pltpu.VMEM((UNIT, D), bf),
            pltpu.VMEM((UNIT, 4 * HEAD), f32),
            dma((5,)), dma((8,)), dma((8,)), dma((X - 1,)), dma((X - 1,)),
            dma((Z - 1,)), dma((Z - 1,)), dma((7,)), dma((7,)),
        ],
        compiler_params=pltpu.CompilerParams(collective_id=0, has_side_effects=True, vmem_limit_bytes=40 << 20),
    )(
        latents, context, cond.reshape(1, -1), ctx_cond.reshape(1, -1), mod_weight, wq, wk, wv,
        q_gain.reshape(1, -1), k_gain.reshape(1, -1), cos_r, sin_r, cos_c, sin_c,
    )


def flash_kernel(steps, sub, q_ref, kv_ref, o_ref, m_ref, acc_ref):
    i = pl.program_id(0)
    keys = kv_ref.shape[0]
    rows = q_ref.shape[0]

    @pl.when(i == 0)
    def _():
        m_ref[...] = jnp.full_like(m_ref, -1e30)
        acc_ref[...] = jnp.zeros_like(acc_ref)

    k = kv_ref[:, :HEAD]
    row = lax.broadcasted_iota(jnp.int32, (keys, HEAD), 0) + i * keys
    ones = jnp.where(lax.rem(row, UNIT) < CTX_ROWS, LIFT, 1.0).astype(jnp.bfloat16)
    v = jnp.concatenate([kv_ref[:, HEAD:], ones], axis=1)
    for h in range(2):
        for r in range(0, rows, sub):
            at = pl.ds(h * rows + r, sub)
            s = lax.dot_general(
                q_ref[r : r + sub, h * HEAD : (h + 1) * HEAD], k, (((1,), (1,)), ((), ())),
                preferred_element_type=jnp.float32,
            )
            m_old = m_ref[at, :]
            m_new = jnp.maximum(m_old, jnp.max(s, axis=1, keepdims=True))
            p = jnp.exp2((s - m_new[:, :1]) * SCORE_SCALE).astype(jnp.bfloat16)
            fade = jnp.exp2((m_old - m_new) * SCORE_SCALE)
            pv = jnp.dot(p, v, preferred_element_type=jnp.float32)
            acc_ref[at, :HEAD] = acc_ref[at, :HEAD] * fade + pv[:, :HEAD]
            acc_ref[at, HEAD:] = acc_ref[at, HEAD:] * fade + pv[:, HEAD:]
            m_ref[at, :] = m_new

    @pl.when(i == steps - 1)
    def _():
        for h in range(2):
            at = pl.ds(h * rows, rows)
            o_ref[:, h * HEAD : (h + 1) * HEAD] = (acc_ref[at, :HEAD] / acc_ref[at, HEAD:]).astype(jnp.bfloat16)


def flash(q, kv):
    keys, sub = 1536, 128
    steps = kv.shape[0] // keys
    rows = q.shape[0]
    return pl.pallas_call(
        functools.partial(flash_kernel, steps, sub),
        name="flash",
        grid=(steps,),
        in_specs=[
            pl.BlockSpec((rows, 2 * HEAD), lambda i: (0, 0)),
            pl.BlockSpec((keys, 2 * HEAD), lambda i: (i, 0)),
        ],
        out_specs=pl.BlockSpec((rows, 2 * HEAD), lambda i: (0, 0)),
        out_shape=jax.ShapeDtypeStruct((rows, 2 * HEAD), jnp.bfloat16),
        scratch_shapes=[
            pltpu.VMEM((2 * rows, HEAD), jnp.float32),
            pltpu.VMEM((2 * rows, 2 * HEAD), jnp.float32),
        ],
        compiler_params=pltpu.CompilerParams(vmem_limit_bytes=40 << 20),
        cost_estimate=pl.CostEstimate(flops=18_000_000_000, bytes_accessed=9_000_000, transcendentals=17_000_000),
    )(q, kv)


def body(
    latents, context, cond, ctx_cond, mod_weight, query_weight, key_matrix, value_matrix,
    out_weight, query_gain, key_gain,
):
    q, kv, gate = front(
        latents, context, cond, ctx_cond, mod_weight, query_weight, key_matrix, value_matrix,
        query_gain, key_gain,
    )
    attended = flash(q, lax.all_gather(kv, SP, axis=0, tiled=True))
    rows = lax.all_to_all(attended, TP, split_axis=0, concat_axis=1, tiled=True)
    weight = lax.all_gather(out_weight, TP, axis=0, tiled=True)
    mixed = jnp.dot(rows, weight, preferred_element_type=jnp.float32)
    mixed = mixed * lax.rsqrt(jnp.mean(mixed * mixed, axis=-1, keepdims=True) + NORM_EPS)
    return (latents.astype(jnp.float32) + gate * mixed).astype(jnp.bfloat16)


def solution(mesh):
    torus = Mesh(mesh.devices.reshape(Z, X, Y, C), AXES)
    placed = (
        P(AXES, None), P(SP, None), P(SP), P(SP), P(SP, TP), P(None, TP), P(None, TP), P(None, TP),
        P(TP, None), P(), P(),
    )
    return jax.shard_map(body, mesh=torus, in_specs=placed, out_specs=P(AXES, None), check_vma=False)
```

time: 286 us -> 209 us (0.73)
  blocking collectives: 100 us -> 15.4 us
  Pallas kernels: 0 us -> 58.7 us
  matrix products: 57.2 us -> 5.06 us
  waiting for transfers between devices: 70.3 us -> 99.6 us
  other arithmetic: 22.9 us -> 0.86 us
  local copies, waits for them, and re-layouts: 20.4 us -> 15.4 us
    all_gather x2 -> x0, blocking collectives: 59.9 us -> none  [the longest x1 40.4 us: side_by_side(): filled, at, done = (lax.all_gather(both, axis, axis=dim, tiled=True), 0, [])]
    pallas_call x0 -> x2, Pallas kernels: none -> 58.7 us  [the longest x1 32.6 us: flash(): pl.pallas_call(functools.partial(flash_kernel, steps, sub), name='flash',...]
    dot_general x25 -> x1, matrix products: 57.2 us -> 5.06 us  [body(): mixed = jnp.dot(rows, weight, preferred_element_type=jnp.float32)]
    all_gather x3 -> x2, waiting for transfers between devices: 69.5 us -> 98.9 us  [the longest x1 95.2 us: body(): attended = flash(q, lax.all_gather(kv, SP, axis=0, tiled=True))]
    psum x2 -> x0, blocking collectives: 26.1 us -> none  [over_axes(): value = lax.psum(value, axis)]
    unnamed x14 -> x32, local copies, waits for them, and re-layouts: 0.03 us -> 15.4 us
    reduce_sum x11 -> x0, other arithmetic: 13.1 us -> none  [the longest x8 11.5 us: update(): jnp.sum(weights_now, axis=-1)]
    while x10 -> x0, local copies, waits for them, and re-layouts: 12.8 us -> none  [the longest x2 12.8 us: body(): state_out, _ = lax.scan(one_step, initial, (key_blocks, value_blocks))]
  transfers between devices with their start and end apart: 3 -> 2, of which waited for: 2 -> 2; matrix products, arithmetic and copies ran while one was open for 29% -> 0% of each run, Pallas kernels for 0% -> 16%
where the time goes in v1:
time: 209 us; the launch traced here: 208 us
  waiting for transfers between devices  99.6 us (48%)
  Pallas kernels  58.7 us (28%)
  local copies, waits for them, and re-layouts  15.4 us (7%)
  blocking collectives  15.4 us (7%)
  between operations  13.5 us (6%)
  matrix products  5.06 us (2%)
    all_gather x1, waiting for transfers between devices, body(): attended = flash(q, lax.all_gather(kv, SP, axis=0, tiled=True))  95.2 us
    pallas_call x1, Pallas kernels, flash(): pl.pallas_call(functools.partial(flash_kernel, steps, sub), name='flash',...  32.6 us
    pallas_call x1, Pallas kernels, front(): pl.pallas_call(front_kernel, name='front', out_shape=(jax.ShapeDtypeStruc...  26 us
    unnamed x32, local copies, waits for them, and re-layouts  15.4 us
    all_to_all x1, blocking collectives, body(): rows = lax.all_to_all(attended, TP, split_axis=0, concat_axis=1, tiled=True)  15.4 us
    dot_general x1, matrix products, body(): mixed = jnp.dot(rows, weight, preferred_element_type=jnp.float32)  5.06 us
  transfers between devices with their start and end apart: 2, of which 2 were waited for; matrix products, arithmetic and copies ran while one was open for 0% of the time, Pallas kernels for 16%

profile of v1, /device:TPU:1, one launch (start us, length us, event | category | flops | bytes accessed | tf_op | source)
XLA Modules:
  0.0 208.5 jit_solution(651191054712932945)
XLA Ops:
  6.5 0.0 all-gather.3.cloned.1.call-start
  6.5 0.0 copy-start
  6.5 1.2 copy-done
  7.8 0.0 copy-start.1
  7.8 0.9 copy-done.1
  8.7 0.0 copy-start.3
  8.7 1.0 copy-done.3
  9.8 0.0 copy-start.4
  9.8 1.0 copy-done.4
  10.8 0.0 copy-start.5
  10.8 0.9 copy-done.5
  11.7 0.0 copy-start.6
  11.7 0.9 copy-done.6
  12.6 0.0 copy-start.7
  12.6 0.9 copy-done.7
  13.5 0.0 copy-start.8
  13.5 0.8 copy-done.8
  14.4 0.0 copy-start.9
  14.4 0.8 copy-done.9
  15.1 0.0 copy-start.10
  15.1 0.8 copy-done.10
  15.9 0.0 copy-start.11
  15.9 0.7 copy-done.11
  16.5 0.0 copy-start.12
  16.5 0.7 copy-done.12
  17.2 0.0 copy-start.13
  17.2 0.7 copy-done.13
  17.9 0.0 copy-start.14
  17.9 0.7 copy-done.14
  18.5 26.0 %front.1 = (bf16[512,256]{1,0:T(8,128)(2,1)S(1)}, bf16[528,256]{1,0:T(8,128)(2,1)}, f32[1,2048]{1,0:T(1,128)S(1)}) custom-call(bf16[64,2048]{1,0:T(8,128)(2,1)S(1)} %copy-done.1, bf16[16,2048]{1,0:T(8,128)(2,1)S(1)} %copy-done.8, f32[1,64]{1,0:T(1,128)S(1)} %bitcast.13, f32[1,64]{1,0:T(1,128)S(1)} %bitcast.14, f32[64,768]{1,0:T(8,128)S(1)} %copy-done.5, ...), custom_call_target="tpu_custom_call" | custom-call | tf_op jit(solution)/shard_map/front/pallas_call | solution.py:216
  44.5 0.0 all-gather.3.cloned.1.call-update
  44.6 0.0 all-gather.5.cloned.1.call-start
  44.6 0.7 all-gather.5.cloned.1.call-update
  45.3 95.2 %all-gather.3.cloned.1.call-done.kv_ref = bf16[16896,256]{1,0:T(8,128)(2,1)} async-done(((bf16[528,256]{1,0:T(8,128)(2,1)}), bf16[16896,256]{1,0:T(8,128)(2,1)}) %all-gather.3.cloned.1.call-update) | async-done | bytes 8650768 | tf_op jit(solution)/shard_map/all_gather | solution.py:316
  140.5 0.0 copy-start.15
  140.5 3.5 %copy-done.15 = bf16[16896,256]{1,0:T(8,128)(2,1)S(1)} copy-done((bf16[16896,256]{1,0:T(8,128)(2,1)S(1)}, bf16[16896,256]{1,0:T(8,128)(2,1)}, u32[]{:S(2)}) %copy-start.15) | copy-done | bytes 8650776
  144.0 32.6 %flash.1 = bf16[512,256]{1,0:T(8,128)(2,1)S(1)} custom-call(bf16[512,256]{1,0:T(8,128)(2,1)S(1)} %get-tuple-element.9.q_ref, bf16[16896,256]{1,0:T(8,128)(2,1)S(1)} %copy-done.15), custom_call_target="tpu_custom_call" | custom-call | flops 17999998976 | bytes 9000000 | tf_op jit(solution)/shard_map/flash/pallas_call | solution.py:289
  176.6 15.4 %all_to_all.19 = bf16[8,64,256]{2,1,0:T(8,128)(2,1)S(1)} all-to-all(bf16[8,64,256]{2,1,0:T(8,128)(2,1)S(1)} %bitcast.11), channel_id=1, replica_groups=mesh['z'=8,'x'=4,'y'=4,'c'=2] {'y','c'}, dimensions={0} | all-to-all | bytes 524288 | tf_op jit(solution)/shard_map/all_to_all | solution.py:317
  192.0 0.0 copy-start.2
  192.0 3.7 %all-gather.5.cloned.1.call-done = bf16[2048,2048]{1,0:T(8,128)(2,1)} async-done(((bf16[256,2048]{1,0:T(8,128)(2,1)}), bf16[2048,2048]{1,0:T(8,128)(2,1)}) %all-gather.5.cloned.1.call-update) | async-done | bytes 8388624 | tf_op jit(solution)/shard_map/all_gather | solution.py:318
  195.7 5.1 %multiply_reduce_fusion = (f32[64]{0:T(128)S(1)}, f32[64,2048]{1,0:T(8,128)S(1)}) fusion(bf16[64,2048]{1,0:T(8,128)(2,1)S(1)} %bitcast.17, bf16[2048,2048]{1,0:T(8,128)(2,1)} %all-gather.5.cloned.1.call-done), kind=kOutput, calls=%fused_computation.1 | convolution fusion | flops 537132992 | bytes 9175296 | tf_op jit(solution)/shard_map/dot_general | solution.py:319
  200.8 0.0 copy-done.2
  200.8 0.9 add_convert_fusion
  (2 shorter events, 0.0 us)
Async XLA Ops:
  6.5 134.0 %all-gather.3.cloned.1.call-start = ((), (), s32[]{:S(2)}) async-start(), calls=%async_computation.1 | async-start | bytes 8921088 | tf_op jit(solution)/shard_map/all_gather | solution.py:316
  6.5 1.2 copy-start
  7.8 0.9 copy-start.1
  8.7 1.0 copy-start.3
  9.8 1.0 copy-start.4
  10.8 0.9 copy-start.5
  11.7 0.9 copy-start.6
  12.6 0.9 copy-start.7
  13.5 0.8 copy-start.8
  14.4 0.8 copy-start.9
  15.1 0.8 copy-start.10
  15.9 0.7 copy-start.11
  16.5 0.7 copy-start.12
  17.2 0.7 copy-start.13
  17.9 0.7 copy-start.14
  44.6 151.1 %all-gather.5.cloned.1.call-start = ((), (), s32[]{:S(2)}) async-start(), calls=%async_computation.2 | async-start | bytes 9437184 | tf_op jit(solution)/shard_map/all_gather | solution.py:318
  140.5 3.5 %copy-start.15 = (bf16[16896,256]{1,0:T(8,128)(2,1)S(1)}, bf16[16896,256]{1,0:T(8,128)(2,1)}, u32[]{:S(2)}) copy-start(bf16[16896,256]{1,0:T(8,128)(2,1)} %all-gather.3.cloned.1.call-done.kv_ref) | copy-start | bytes 25952260
  192.0 8.8 %copy-start.2 = (bf16[64,2048]{1,0:T(8,128)(2,1)S(1)}, bf16[64,2048]{1,0:T(8,128)(2,1)}, u32[]{:S(2)}) copy-start(bf16[64,2048]{1,0:T(8,128)(2,1)} %lat.1) | copy-start | bytes 786436
Sparse Core Ops, SparseCore 0:
  44.7 95.7 all-gather.2
  142.4 53.2 all-gather.4

commit v2 on v1

--- a/solution.py
+++ b/solution.py
@@ -245,64 +245,357 @@
     )
 
 
-def flash_kernel(steps, sub, q_ref, kv_ref, o_ref, m_ref, acc_ref):
-    i = pl.program_id(0)
-    keys = kv_ref.shape[0]
-    rows = q_ref.shape[0]
-
-    @pl.when(i == 0)
+H1 = 240
+H2 = UNIT - H1
+CHUNK = 1408
+CHUNKS = TOTAL_KEYS // CHUNK
+SUB = 128
+
+
+def unit_order():
+    order = [(0, "own", s) for s in (0, 1)] + [(0, "nbr", s) for s in (0, 1)]
+    for t, col in ((1, "own"), (2, "own"), (1, "nbr"), (3, "own"), (2, "nbr"), (4, "own"), (3, "nbr"), (4, "nbr")):
+        for s in (0, 1):
+            order += [(d, col, s) for d in ((t, -t) if t < 4 else (4,))]
+    return {u: i for i, u in enumerate(order)}
+
+
+ORDER = unit_order()
+DS = (0, 1, -1, 2, -2, 3, -3, 4)
+KINDS = ("own", "nbr", "h2")
+
+
+def main_kernel(
+    q_in, kv_in, ow_in, lat_in, gate_in, out,
+    keys, qb, ones, m_ref, acc, att, got, ow, lat, gate, mixed,
+    loc, z_send, z_recv, x_send, x_recv, d_send, d_recv, o_send, o_recv, s_send, s_recv, a_send, a_recv,
+):
+    z, x, y, c = coords()
+    me = y * C + c
+    pair = x + 1 - 2 * lax.rem(x, 2)
+    is_a = lax.rem((x + 1) // 2, 2)
+    swapped = is_a == c
+    row_x = x + (pair - x) * (1 - lax.rem(is_a + c, 2))
+    head = y * C + 1 - is_a
+    up, down, far = lax.rem(y + 1, Y), lax.rem(y + Y - 1, Y), lax.rem(y + 2, Y)
+    sib = (z, x, y, 1 - c)
+    partner = (z, pair, y, 1 - c)
+    nbr = (z, X - 1 - x, y, c)
+    z_up, z_down = (lax.rem(z + 1, Z), x, y, c), (lax.rem(z + Z - 1, Z), x, y, c)
+    y_up, y_down = (z, x, up, c), (z, x, down, c)
+    rel = [(ry, rc) for ry in range(Y) for rc in range(C)]
+    flip = 1 - 2 * c
+
+    local = [
+        pltpu.make_async_copy(lat_in, lat, loc.at[2]),
+        pltpu.make_async_copy(gate_in, gate, loc.at[3]),
+        pltpu.make_async_copy(ow_in, ow.at[me], loc.at[4]),
+    ]
+    for copy in local:
+        copy.start()
+    q_local = pltpu.make_async_copy(q_in, qb, loc.at[0])
+    kv_local = pltpu.make_async_copy(kv_in, keys.at[pl.ds(0, UNIT)], loc.at[1])
+
+    @pl.when(jnp.logical_not(swapped))
     def _():
-        m_ref[...] = jnp.full_like(m_ref, -1e30)
-        acc_ref[...] = jnp.zeros_like(acc_ref)
-
-    k = kv_ref[:, :HEAD]
-    row = lax.broadcasted_iota(jnp.int32, (keys, HEAD), 0) + i * keys
-    ones = jnp.where(lax.rem(row, UNIT) < CTX_ROWS, LIFT, 1.0).astype(jnp.bfloat16)
-    v = jnp.concatenate([kv_ref[:, HEAD:], ones], axis=1)
+        kv_local.start()
+        q_local.start()
+
+    meet(
+        [(z, x, lax.rem(y + ry, Y), c + rc * flip) for ry, rc in rel[1:]]
+        + [(z, pair, lax.rem(y + ry, Y), c + rc * flip) for ry, rc in rel]
+        + [z_up, z_down, nbr]
+    )
+
+    def at(d, col, s, lo, n):
+        return keys.at[pl.ds(ORDER[(d, col, s)] * UNIT + lo, n)]
+
+    def swap_kv():
+        return remote(kv_in, keys.at[pl.ds(0, UNIT)], s_send.at[0], s_recv.at[0], partner)
+
+    def swap_q():
+        return remote(q_in, qb, s_send.at[1], s_recv.at[1], partner)
+
+    def ring(direction, t, kind):
+        col = "nbr" if kind == "nbr" else "own"
+        lo, n = (H1, H2) if kind == "h2" else (0, H1)
+        if kind == "h2" and t == 4:
+            n = H2 // 2
+            lo = lo if direction > 0 else lo + n
+        dst = 4 if t == 4 else direction * t
+        i = (0 if direction > 0 else 12) + (t - 1) * 3 + KINDS.index(kind)
+        return remote(
+            at(direction * (t - 1), col, 0, lo, n), at(dst, col, 0, lo, n), z_send.at[i], z_recv.at[i],
+            z_up if direction > 0 else z_down,
+        )
+
+    def used(direction, t, kind):
+        return t < 4 or kind == "h2" or (kind == "own") == (direction > 0)
+
+    def cross(d):
+        i = DS.index(d)
+        return remote(at(d, "own", 0, H1, H2), at(d, "nbr", 0, H1, H2), x_send.at[i], x_recv.at[i], nbr)
+
+    def cross_h1():
+        return remote(at(0, "own", 0, 0, H1), at(0, "nbr", 0, 0, H1), x_send.at[8], x_recv.at[8], nbr)
+
+    def share(d, col):
+        i = DS.index(d) + (0 if col == "own" else 8)
+        return remote(at(d, col, 0, 0, UNIT), at(d, col, 1, 0, UNIT), d_send.at[i], d_recv.at[i], sib)
+
+    half = 2 * HEAD // 2
+
+    def weight(i):
+        who = [
+            (ow_in, me, 0, 2 * half, y_up), (ow_in, me, 0, 2 * half, y_down), (ow_in, me, 0, 2 * half, sib),
+            (None, down * C + c, 0, half, y_up), (None, up * C + c, half, half, y_down),
+            (None, down * C + c, 0, 2 * half, sib), (None, up * C + c, 0, 2 * half, sib),
+            (None, far * C + c, 0, 2 * half, sib),
+        ][i]
+        src, slot, lo, n, dev = who
+        dst = ow.at[slot, pl.ds(lo, n)]
+        return remote(dst if src is None else src, dst, o_send.at[i], o_recv.at[i], dev)
+
+    def on_ring(t, kind):
+        for direction in (1, -1):
+            if used(direction, t, kind):
+                ring(direction, t, kind).wait_recv()
+            if t < 4 and used(direction, t + 1, kind):
+                ring(direction, t + 1, kind).start()
+
+    def begin():
+        for i in range(3):
+            weight(i).start()
+
+        @pl.when(swapped)
+        def _():
+            swap_kv().start()
+            swap_q().start()
+            swap_kv().wait_recv()
+
+        @pl.when(jnp.logical_not(swapped))
+        def _():
+            kv_local.wait()
+
+        cross_h1().start()
+        for kind in ("own", "h2"):
+            for direction in (1, -1):
+                ring(direction, 1, kind).start()
+        share(0, "own").start()
+        cross(0).start()
+
+    def own_done(t):
+        on_ring(t, "h2")
+        for d in ((t, -t) if t < 4 else (4,)):
+            cross(d).start()
+            share(d, "own").start()
+
+    def nbr_done(t):
+        for d in ((t, -t) if 0 < t < 4 else (t,)):
+            cross(d).wait_recv()
+            share(d, "nbr").start()
+
+    def shared(t, col):
+        for d in ((t, -t) if 0 < t < 4 else (t,)):
+            share(d, col).wait_recv()
+
+    def step0():
+        cross_h1().wait_recv()
+        for direction in (1, -1):
+            ring(direction, 1, "nbr").start()
+        on_ring(1, "own")
+        nbr_done(0)
+        own_done(1)
+
+        @pl.when(swapped)
+        def _():
+            swap_q().wait_recv()
+
+        @pl.when(jnp.logical_not(swapped))
+        def _():
+            q_local.wait()
+
+        shared(0, "own")
+
+    def step1():
+        shared(0, "nbr")
+        on_ring(1, "nbr")
+
+    def step2():
+        shared(1, "own")
+        on_ring(2, "own")
+
+    def step3():
+        own_done(2)
+        shared(2, "own")
+
+    def step4():
+        nbr_done(1)
+        on_ring(2, "nbr")
+
+    def step5():
+        shared(1, "nbr")
+        on_ring(3, "own")
+
+    def step6():
+        own_done(3)
+        shared(3, "own")
+
+    def step7():
+        nbr_done(2)
+        on_ring(3, "nbr")
+        for i in (0, 1):
+            weight(i).wait_recv()
+        for i in (3, 4, 5, 6):
+            weight(i).start()
+
+    def step8():
+        shared(2, "nbr")
+
+    def step9():
+        on_ring(4, "own")
+        own_done(4)
+        nbr_done(3)
+        shared(4, "own")
+
+    def step10():
+        shared(3, "nbr")
+
+    def step11():
+        on_ring(4, "nbr")
+        nbr_done(4)
+        shared(4, "nbr")
+
+    steps = (step0, step1, step2, step3, step4, step5, step6, step7, step8, step9, step10, step11)
+
+    begin()
+    ones[...] = jnp.ones_like(ones)
+    for u in range(3 * CHUNK // UNIT):
+        ones[UNIT * u : UNIT * u + CTX_ROWS, :] = jnp.full((CTX_ROWS, HEAD), LIFT, jnp.bfloat16)
+    m_ref[...] = jnp.full_like(m_ref, -1e30)
+    acc[...] = jnp.zeros_like(acc)
+
+    def chunk(i, carry):
+        for j, step in enumerate(steps):
+            pl.when(i == j)(step)
+        rows = pl.ds(pl.multiple_of(i * CHUNK, CHUNK), CHUNK)
+        k = keys[rows, :HEAD]
+        w = ones[pl.ds(pl.multiple_of(lax.rem(i, 3) * CHUNK, CHUNK), CHUNK), :]
+        v = jnp.concatenate([keys[rows, HEAD:], w], axis=1)
+        for h in range(2):
+            for r in range(0, GROUP_ROWS, SUB):
+                sl = pl.ds(h * GROUP_ROWS + r, SUB)
+                s = lax.dot_general(
+                    qb[r : r + SUB, h * HEAD : (h + 1) * HEAD], k, (((1,), (1,)), ((), ())),
+                    preferred_element_type=jnp.float32,
+                )
+                m_old = m_ref[sl, :]
+                m_new = jnp.maximum(m_old, jnp.max(s, axis=1, keepdims=True))
+                p = jnp.exp2((s - m_new[:, :1]) * SCORE_SCALE).astype(jnp.bfloat16)
+                fade = jnp.exp2((m_old - m_new) * SCORE_SCALE)
+                pv = jnp.dot(p, v, preferred_element_type=jnp.float32)
+                acc[sl, :HEAD] = acc[sl, :HEAD] * fade + pv[:, :HEAD]
+                acc[sl, HEAD:] = acc[sl, HEAD:] * fade + pv[:, HEAD:]
+                m_ref[sl, :] = m_new
+        return carry
+
+    lax.fori_loop(0, CHUNKS, chunk, 0)
+
+    for i in (3, 4):
+        weight(i).wait_recv()
+    weight(7).start()
     for h in range(2):
-        for r in range(0, rows, sub):
-            at = pl.ds(h * rows + r, sub)
-            s = lax.dot_general(
-                q_ref[r : r + sub, h * HEAD : (h + 1) * HEAD], k, (((1,), (1,)), ((), ())),
-                preferred_element_type=jnp.float32,
+        sl = pl.ds(h * GROUP_ROWS, GROUP_ROWS)
+        att[:, h * HEAD : (h + 1) * HEAD] = (acc[sl, :HEAD] / acc[sl, HEAD:]).astype(jnp.bfloat16)
+
+    def hand(i):
+        ry, rc = rel[i]
+        yy, cc = lax.rem(y + ry, Y), c + rc * flip
+        src = att.at[pl.ds(pl.multiple_of((yy * C + cc) * ROWS, ROWS), ROWS)]
+        return remote(src, got.at[head], a_send.at[i], a_recv.at[head], (z, row_x, yy, cc))
+
+    for i in range(1, Y * C):
+        hand(i).start()
+
+    @pl.when(swapped)
+    def _():
+        hand(0).start()
+
+    @pl.when(jnp.logical_not(swapped))
+    def _():
+        got[head] = att[pl.ds(pl.multiple_of(me * ROWS, ROWS), ROWS), :]
+
+    for copy in local:
+        copy.wait()
+    for i in (2, 5, 6, 7):
+        weight(i).wait_recv()
+    for j in range(Y * C):
+
+        @pl.when(jnp.logical_or(swapped, head != j))
+        def _():
+            remote(att.at[pl.ds(0, ROWS)], got.at[j], a_send.at[0], a_recv.at[j], sib).wait_recv()
+
+    rows = jnp.concatenate([got[j] for j in range(Y * C)], axis=1)
+    for n in range(0, D, 512):
+        total = jnp.zeros((ROWS, 512), jnp.float32)
+        for j in range(Y * C):
+            total = total + jnp.dot(
+                rows[:, j * 2 * HEAD : (j + 1) * 2 * HEAD], ow[j, :, n : n + 512], preferred_element_type=jnp.float32
             )
-            m_old = m_ref[at, :]
-            m_new = jnp.maximum(m_old, jnp.max(s, axis=1, keepdims=True))
-            p = jnp.exp2((s - m_new[:, :1]) * SCORE_SCALE).astype(jnp.bfloat16)
-            fade = jnp.exp2((m_old - m_new) * SCORE_SCALE)
-            pv = jnp.dot(p, v, preferred_element_type=jnp.float32)
-            acc_ref[at, :HEAD] = acc_ref[at, :HEAD] * fade + pv[:, :HEAD]
-            acc_ref[at, HEAD:] = acc_ref[at, HEAD:] * fade + pv[:, HEAD:]
-            m_ref[at, :] = m_new
-
-    @pl.when(i == steps - 1)
+        mixed[:, n : n + 512] = total
+    v = mixed[...]
+    v = v * lax.rsqrt(jnp.mean(v * v, axis=-1, keepdims=True) + NORM_EPS)
+    out[...] = (lat[...].astype(jnp.float32) + gate[...] * v).astype(jnp.bfloat16)
+
+    for kind in KINDS:
+        for t in range(1, 5):
+            for direction in (1, -1):
+                if used(direction, t, kind):
+                    ring(direction, t, kind).wait_send()
+    for d in DS:
+        cross(d).wait_send()
+        share(d, "own").wait_send()
+        share(d, "nbr").wait_send()
+    cross_h1().wait_send()
+    for i in range(8):
+        weight(i).wait_send()
+    for i in range(1, Y * C):
+        hand(i).wait_send()
+
+    @pl.when(swapped)
     def _():
-        for h in range(2):
-            at = pl.ds(h * rows, rows)
-            o_ref[:, h * HEAD : (h + 1) * HEAD] = (acc_ref[at, :HEAD] / acc_ref[at, HEAD:]).astype(jnp.bfloat16)
-
-
-def flash(q, kv):
-    keys, sub = 1536, 128
-    steps = kv.shape[0] // keys
-    rows = q.shape[0]
+        hand(0).wait_send()
+        swap_kv().wait_send()
+        swap_q().wait_send()
+
+
+def attend(q, kv, out_weight, latents, gate):
+    hbm = pl.BlockSpec(memory_space=pltpu.HBM)
+    bf, f32 = jnp.bfloat16, jnp.float32
+    dma = pltpu.SemaphoreType.DMA
     return pl.pallas_call(
-        functools.partial(flash_kernel, steps, sub),
-        name="flash",
-        grid=(steps,),
-        in_specs=[
-            pl.BlockSpec((rows, 2 * HEAD), lambda i: (0, 0)),
-            pl.BlockSpec((keys, 2 * HEAD), lambda i: (i, 0)),
+        main_kernel,
+        name="attend",
+        out_shape=jax.ShapeDtypeStruct((ROWS, D), bf),
+        in_specs=[hbm] * 5,
+        out_specs=pl.BlockSpec(memory_space=pltpu.VMEM),
+        scratch_shapes=[
+            pltpu.VMEM((TOTAL_KEYS, 2 * HEAD), bf),
+            pltpu.VMEM((GROUP_ROWS, 2 * HEAD), bf),
+            pltpu.VMEM((3 * CHUNK, HEAD), bf),
+            pltpu.VMEM((2 * GROUP_ROWS, HEAD), f32),
+            pltpu.VMEM((2 * GROUP_ROWS, 2 * HEAD), f32),
+            pltpu.VMEM((GROUP_ROWS, 2 * HEAD), bf),
+            pltpu.VMEM((Y * C, ROWS, 2 * HEAD), bf),
+            pltpu.VMEM((Y * C, 2 * HEAD, D), bf),
+            pltpu.VMEM((ROWS, D), bf),
+            pltpu.VMEM((1, D), f32),
+            pltpu.VMEM((ROWS, D), f32),
+            dma((5,)), dma((24,)), dma((24,)), dma((9,)), dma((9,)), dma((16,)), dma((16,)),
+            dma((8,)), dma((8,)), dma((2,)), dma((2,)), dma((8,)), dma((8,)),
         ],
-        out_specs=pl.BlockSpec((rows, 2 * HEAD), lambda i: (0, 0)),
-        out_shape=jax.ShapeDtypeStruct((rows, 2 * HEAD), jnp.bfloat16),
-        scratch_shapes=[
-            pltpu.VMEM((2 * rows, HEAD), jnp.float32),
-            pltpu.VMEM((2 * rows, 2 * HEAD), jnp.float32),
-        ],
-        compiler_params=pltpu.CompilerParams(vmem_limit_bytes=40 << 20),
-        cost_estimate=pl.CostEstimate(flops=18_000_000_000, bytes_accessed=9_000_000, transcendentals=17_000_000),
-    )(q, kv)
+        compiler_params=pltpu.CompilerParams(collective_id=1, has_side_effects=True, vmem_limit_bytes=60 << 20),
+    )(q, kv, out_weight, latents, gate)
 
 
 def body(
@@ -313,12 +606,7 @@
         latents, context, cond, ctx_cond, mod_weight, query_weight, key_matrix, value_matrix,
         query_gain, key_gain,
     )
-    attended = flash(q, lax.all_gather(kv, SP, axis=0, tiled=True))
-    rows = lax.all_to_all(attended, TP, split_axis=0, concat_axis=1, tiled=True)
-    weight = lax.all_gather(out_weight, TP, axis=0, tiled=True)
-    mixed = jnp.dot(rows, weight, preferred_element_type=jnp.float32)
-    mixed = mixed * lax.rsqrt(jnp.mean(mixed * mixed, axis=-1, keepdims=True) + NORM_EPS)
-    return (latents.astype(jnp.float32) + gate * mixed).astype(jnp.bfloat16)
+    return attend(q, kv, out_weight, latents, gate)
 
 
 def solution(mesh):

time: 209 us -> 104 us (0.50)
  waiting for transfers between devices: 99.6 us -> 0 us
  Pallas kernels: 58.7 us -> 89.7 us
  blocking collectives: 15.4 us -> 0 us
  between operations: 13.5 us -> 0.05 us
  matrix products: 5.06 us -> 0 us
    all_gather x2 -> x0, waiting for transfers between devices: 98.9 us -> none  [the longest x1 95.2 us: body(): attended = flash(q, lax.all_gather(kv, SP, axis=0, tiled=True))]
    pallas_call x1, Pallas kernels: 32.6 us -> 64.3 us  [attend(): pl.pallas_call(main_kernel, name='attend', out_shape=jax.ShapeDtypeStruct...]
    all_to_all x1 -> x0, blocking collectives: 15.4 us -> none  [body(): rows = lax.all_to_all(attended, TP, split_axis=0, concat_axis=1, tiled=True)]
    dot_general x1 -> x0, matrix products: 5.06 us -> none  [body(): mixed = jnp.dot(rows, weight, preferred_element_type=jnp.float32)]
    unnamed x32 -> x35, local copies, waits for them, and re-layouts: 15.4 us -> 13.7 us
  transfers between devices with their start and end apart: 2 -> 0, of which waited for: 2 -> 0; matrix products, arithmetic and copies ran while one was open for 0% -> 0% of each run, Pallas kernels for 16% -> 0%
where the time goes in v2:
time: 104 us; the launch traced here: 103 us
  Pallas kernels  89.7 us (86%)
  local copies, waits for them, and re-layouts  13.7 us (13%)
    pallas_call x1, Pallas kernels, attend(): pl.pallas_call(main_kernel, name='attend', out_shape=jax.ShapeDtypeStruct...  64.3 us
    pallas_call x1, Pallas kernels, front(): pl.pallas_call(front_kernel, name='front', out_shape=(jax.ShapeDtypeStruc...  25.3 us
    unnamed x35, local copies, waits for them, and re-layouts  13.7 us

profile of v2, /device:TPU:1, one launch (start us, length us, event | category | flops | bytes accessed | tf_op | source)
XLA Modules:
  0.0 103.4 jit_solution(17878684520607221829)
XLA Ops:
  0.0 0.0 copy-start.16
  0.0 0.0 copy-start.13
  0.0 0.0 copy-start.14
  0.0 0.0 copy-start.15
  0.0 0.6 copy-done.16
  0.7 0.0 copy-done.13
  0.7 0.0 copy-done.14
  0.7 0.0 copy-done.15
  0.7 0.0 copy-start
  0.7 1.2 %copy-done = bf16[2048,256]{1,0:T(8,128)(2,1)S(1)} copy-done((bf16[2048,256]{1,0:T(8,128)(2,1)S(1)}, bf16[2048,256]{1,0:T(8,128)(2,1)}, u32[]{:S(2)}) %copy-start) | copy-done | bytes 1048600
  1.9 0.0 copy-start.1
  1.9 0.9 copy-done.1
  2.9 0.0 copy-start.2
  2.9 1.0 %copy-done.2 = bf16[2048,128]{1,0:T(8,128)(2,1)S(1)} copy-done((bf16[2048,128]{1,0:T(8,128)(2,1)S(1)}, bf16[2048,128]{1,0:T(8,128)(2,1)}, u32[]{:S(2)}) %copy-start.2) | copy-done | bytes 524312
  3.9 0.0 copy-start.3
  3.9 1.0 %copy-done.3 = bf16[2048,128]{1,0:T(8,128)(2,1)S(1)} copy-done((bf16[2048,128]{1,0:T(8,128)(2,1)S(1)}, bf16[2048,128]{1,0:T(8,128)(2,1)}, u32[]{:S(2)}) %copy-start.3) | copy-done | bytes 524312
  5.0 0.0 copy-start.6
  5.0 0.9 copy-done.6
  5.9 0.0 copy-start.7
  5.9 0.9 copy-done.7
  6.8 0.0 copy-start.8
  6.8 0.9 copy-done.8
  7.7 0.0 copy-start.9
  7.7 0.8 copy-done.9
  8.5 0.0 copy-start.10
  8.5 0.8 copy-done.10
  9.3 0.0 copy-start.11
  9.3 0.8 copy-done.11
  10.1 25.3 %front.1 = (bf16[512,256]{1,0:T(8,128)(2,1)S(1)}, bf16[528,256]{1,0:T(8,128)(2,1)S(1)}, f32[1,2048]{1,0:T(1,128)S(1)}) custom-call(bf16[64,2048]{1,0:T(8,128)(2,1)S(1)} %copy-done.1, bf16[16,2048]{1,0:T(8,128)(2,1)S(1)} %copy-done.9, f32[1,64]{1,0:T(1,128)S(1)} %bitcast.4, f32[1,64]{1,0:T(1,128)S(1)} %bitcast.5, f32[64,768]{1,0:T(8,128)S(1)} %copy-done.6, ...), custom_call_target="tpu_custom_call" | custom-call | tf_op jit(solution)/shard_map/front/pallas_call | solution.py:216
  35.4 0.0 copy-start.4
  35.4 0.7 copy-done.4
  36.1 0.0 copy-start.5
  36.1 0.7 copy-done.5
  36.8 0.0 copy-start.12
  36.8 0.6 copy-done.12
  37.4 64.3 %attend.1 = bf16[64,2048]{1,0:T(8,128)(2,1)} custom-call(bf16[512,256]{1,0:T(8,128)(2,1)} %copy-done.5, bf16[528,256]{1,0:T(8,128)(2,1)} %copy-done.4, bf16[256,2048]{1,0:T(8,128)(2,1)} %ow_in.1, bf16[64,2048]{1,0:T(8,128)(2,1)} %lat_in.1, f32[1,2048]{1,0:T(1,128)} %copy-done.12), custom_call_target="tpu_custom_call" | custom-call | tf_op jit(solution)/shard_map/attend/pallas_call | solution.py:576
  101.7 1.7 %copy.17 = bf16[64,2048]{1,0:T(8,128)(2,1)} copy(bf16[64,2048]{1,0:T(8,128)(2,1)} %attend.1) | data formatting | bytes 524288
Async XLA Ops:
  0.0 0.7 copy-start.16
  0.0 0.7 copy-start.13
  0.0 0.7 copy-start.14
  0.0 0.7 copy-start.15
  0.7 1.2 %copy-start = (bf16[2048,256]{1,0:T(8,128)(2,1)S(1)}, bf16[2048,256]{1,0:T(8,128)(2,1)}, u32[]{:S(2)}) copy-start(bf16[2048,256]{1,0:T(8,128)(2,1)} %wq.1) | copy-start | bytes 3145732
  1.9 0.9 copy-start.1
  2.9 1.0 %copy-start.2 = (bf16[2048,128]{1,0:T(8,128)(2,1)S(1)}, bf16[2048,128]{1,0:T(8,128)(2,1)}, u32[]{:S(2)}) copy-start(bf16[2048,128]{1,0:T(8,128)(2,1)} %wk.1) | copy-start | bytes 1572868
  3.9 1.0 %copy-start.3 = (bf16[2048,128]{1,0:T(8,128)(2,1)S(1)}, bf16[2048,128]{1,0:T(8,128)(2,1)}, u32[]{:S(2)}) copy-start(bf16[2048,128]{1,0:T(8,128)(2,1)} %wv.1) | copy-start | bytes 1572868
  5.0 0.9 copy-start.6
  5.9 0.9 copy-start.7
  6.8 0.9 copy-start.8
  7.7 0.8 copy-start.9
  8.5 0.8 copy-start.10
  9.3 0.8 copy-start.11
  35.4 0.7 copy-start.4
  36.1 0.7 copy-start.5
  36.8 0.6 copy-start.12

commit v3 on v2

v3 whole, which is shorter than its diff:
```python
import functools
import math

import jax
import jax.numpy as jnp
import numpy as np
from jax import lax
from jax.experimental import pallas as pl
from jax.experimental.pallas import tpu as pltpu
from jax.sharding import Mesh
from jax.sharding import PartitionSpec as P

GRID_W = 64
NORM_EPS = 1e-06
ROPE_BASE = 10000.0
Z, X, Y, C = 8, 4, 4, 2
AXES = ("z", "x", "y", "c")
SP = ("z", "x")
TP = ("y", "c")
MESH = pl.DeviceIdType.MESH
D = 2048
HEAD = 128
ROWS = 64
CTX_ROWS = 16
GROUP_ROWS = ROWS * Y * C
UNIT = CTX_ROWS + GROUP_ROWS
TOTAL_KEYS = UNIT * Z * X
LIFT = 16.0
SCORE_SCALE = HEAD ** (-0.5) * math.log2(math.e)


def coords():
    return tuple(lax.axis_index(a) for a in AXES)


def remote(src, dst, send, recv, dev):
    return pltpu.make_async_remote_copy(
        src_ref=src, dst_ref=dst, send_sem=send, recv_sem=recv, device_id=dev, device_id_type=MESH
    )


def meet(peers):
    barrier = pltpu.get_barrier_semaphore()
    for dev in peers:
        pl.semaphore_signal(barrier, inc=1, device_id=dev, device_id_type=MESH)
    pl.semaphore_wait(barrier, len(peers))


def rope_tables():
    quarter = HEAD // 4
    freq = (np.float32(ROPE_BASE) ** (-np.arange(quarter, dtype=np.float32) / np.float32(quarter))).astype(np.float32)
    lanes = freq[np.arange(HEAD) % quarter]
    sign = np.where(np.arange(HEAD) % (HEAD // 2) < quarter, -1.0, 1.0)
    grid_rows = GROUP_ROWS * Z * X // GRID_W
    row_angle = (np.arange(grid_rows, dtype=np.float32)[:, None] * lanes[None]).astype(np.float64)
    col_angle = (np.arange(GRID_W, dtype=np.float32)[:, None] * lanes[None]).astype(np.float64)
    as32 = lambda a: jnp.asarray(a.astype(np.float32))
    return (
        as32(np.cos(row_angle)),
        as32(np.sin(row_angle) * sign),
        as32(np.cos(col_angle)),
        as32(np.sin(col_angle) * sign),
    )


def column(row):
    n = row.shape[1]
    eye = lax.broadcasted_iota(jnp.int32, (n, n), 0) == lax.broadcasted_iota(jnp.int32, (n, n), 1)
    return jnp.sum(jnp.where(eye, row, 0.0), axis=1, keepdims=True)


H1 = 240
H2 = UNIT - H1
CHUNK = 1408
CHUNKS = TOTAL_KEYS // CHUNK
SUB = 352


def unit_order():
    order = [(0, "own", s) for s in (0, 1)] + [(0, "nbr", s) for s in (0, 1)]
    for t, col in ((1, "own"), (2, "own"), (1, "nbr"), (3, "own"), (2, "nbr"), (4, "own"), (3, "nbr"), (4, "nbr")):
        for s in (0, 1):
            order += [(d, col, s) for d in ((t, -t) if t < 4 else (4,))]
    return {u: i for i, u in enumerate(order)}


ORDER = unit_order()
DS = (0, 1, -1, 2, -2, 3, -3, 4)
KINDS = ("own", "nbr", "h2")


def layer_kernel(
    lat_in, ctx_in, cond_in, ctx_cond_in, modw_in, wq, wk, wv, ow_in, q_gain_in, k_gain_in, cos_r, sin_r, cos_c_in, sin_c_in,
    out,
    lat, ctx, cond, ctx_cond, modw, q_gain, k_gain, cos_c, sin_c, cr, sr,
    xg, wqs, wkv, part, x_in, x_sum, z_in, mod, xn, kvb, qt,
    keys, qb, ones, m_ref, acc, att, got, ow, mixed,
    loc, lat_send, lat_recv, mx_send, mx_recv, mz_send, mz_recv, mt_send, mt_recv,
    z_send, z_recv, x_send, x_recv, d_send, d_recv, o_send, o_recv, s_send, s_recv, a_send, a_recv,
):
    z, x, y, c = coords()
    me = y * C + c
    sp = z * X + x
    pair = x + 1 - 2 * lax.rem(x, 2)
    is_a = lax.rem((x + 1) // 2, 2)
    swapped = is_a == c
    row_x = x + (pair - x) * (1 - lax.rem(is_a + c, 2))
    head = y * C + 1 - is_a
    up, down, far = lax.rem(y + 1, Y), lax.rem(y + Y - 1, Y), lax.rem(y + 2, Y)
    sib = (z, x, y, 1 - c)
    partner = (z, pair, y, 1 - c)
    nbr = (z, X - 1 - x, y, c)
    z_up, z_down = (lax.rem(z + 1, Z), x, y, c), (lax.rem(z + Z - 1, Z), x, y, c)
    y_up, y_down = (z, x, up, c), (z, x, down, c)
    rel = [(ry, rc) for ry in range(Y) for rc in range(C)]
    flip = 1 - 2 * c
    x_peers = [(z, lax.rem(x + r, X), y, c) for r in range(1, X)]
    z_peers = [(lax.rem(z + r, Z), x, y, c) for r in range(1, Z)]
    t_peers = [(z, x, lax.rem(y + ry, Y), c + rc * flip) for ry, rc in rel[1:]]

    loads = [
        pltpu.make_async_copy(src, dst, loc.at[i])
        for i, (src, dst) in enumerate((
            (modw_in, modw), (cond_in, cond), (ctx_cond_in, ctx_cond), (lat_in, lat), (ctx_in, ctx),
            (q_gain_in, q_gain), (k_gain_in, k_gain), (cos_c_in, cos_c), (sin_c_in, sin_c),
            (cos_r.at[pl.ds(sp * 8, 8)], cr), (sin_r.at[pl.ds(sp * 8, 8)], sr),
            (wk, wkv.at[:, pl.ds(0, HEAD)]), (wv, wkv.at[:, pl.ds(HEAD, HEAD)]), (wq, wqs), (ow_in, ow.at[me]),
        ))
    ]
    for copy in loads:
        copy.start()
    meet(x_peers + z_peers + t_peers + [(z, pair, lax.rem(y + ry, Y), c + rc * flip) for ry, rc in rel[1:]])

    lat_sends = []

    def send_lat(i, src, yy, dev, lo=0, n=ROWS):
        copy = remote(src, xg.at[yy * C + c, pl.ds(lo, n)], lat_send.at[i], lat_recv.at[i], dev)
        copy.start()
        lat_sends.append(copy)
        return copy

    c0 = send_lat(0, lat_in, y, y_up)
    c1 = send_lat(1, lat_in, y, y_down)
    c2 = send_lat(2, lat_in, y, sib)
    for copy in loads[:5]:
        copy.wait()

    w = modw[...]
    for r, vec in enumerate((cond, ctx_cond)):
        v = vec[...]
        v = column(v * lax.logistic(v))
        row = jnp.sum(v * w, axis=0, keepdims=True)
        for i in range(6):
            part[r * 6 + i : r * 6 + i + 1, :] = row[:, i * HEAD : (i + 1) * HEAD]
    part[12:16, :] = jnp.zeros((4, HEAD), jnp.float32)

    xs = [remote(part, x_in.at[i], mx_send.at[i], mx_recv.at[i], d) for i, d in enumerate(x_peers)]
    for s in xs:
        s.start()
    xg[me] = lat[...]
    wt = lax.broadcasted_iota(jnp.int32, ones.shape, 1)
    ones[...] = jnp.where(lax.rem(wt, UNIT) < CTX_ROWS, LIFT, 1.0).astype(jnp.bfloat16)
    m_ref[...] = jnp.full_like(m_ref, -1e30)
    acc[...] = jnp.zeros_like(acc)
    for s in xs:
        s.wait_recv()
    x_sum[...] = part[...] + x_in[0] + x_in[1] + x_in[2]
    zs = [remote(x_sum, z_in.at[i], mz_send.at[i], mz_recv.at[i], d) for i, d in enumerate(z_peers)]
    for s in zs:
        s.start()

    hr = ROWS // 2
    c0.wait_recv()
    c3 = send_lat(3, xg.at[down * C + c, pl.ds(0, hr)], down, y_up, 0, hr)
    c5 = send_lat(5, xg.at[down * C + c], down, sib)
    c1.wait_recv()
    c4 = send_lat(4, xg.at[up * C + c, pl.ds(hr, hr)], up, y_down, hr, hr)
    c6 = send_lat(6, xg.at[up * C + c], up, sib)

    for s in zs:
        s.wait_recv()
    total = x_sum[...]
    for i in range(Z - 1):
        total = total + z_in[i]
    mod[me] = total
    ts = [remote(mod.at[me], mod.at[me], mt_send.at[i], mt_recv.at[i], d) for i, d in enumerate(t_peers)]
    for s in ts:
        s.start()
    for copy in loads[5:]:
        copy.wait()
    for s in ts:
        s.wait_recv()

    def mod_row(r, first):
        tiles = [first + t for t in range(D // HEAD)]
        return jnp.concatenate([mod[t // 6, r * 6 + t % 6 : r * 6 + t % 6 + 1, :] for t in tiles], axis=1)

    def modulated(rows, r):
        v = rows.astype(jnp.float32)
        v = v * lax.rsqrt(jnp.mean(v * v, axis=-1, keepdims=True) + NORM_EPS)
        return (v * (1.0 + mod_row(r, 16)) + mod_row(r, 0)).astype(jnp.bfloat16)

    def make_rows(j):
        lo = pl.multiple_of(CTX_ROWS + ROWS * j, CTX_ROWS)
        xn[pl.ds(lo, ROWS), :] = modulated(xg[j], 0)

    xn[:CTX_ROWS, :] = modulated(ctx[...], 1)
    make_rows(me)
    c2.wait_recv()
    make_rows(y * C + 1 - c)
    make_rows(down * C + c)
    make_rows(up * C + c)
    c3.wait_recv()
    c4.wait_recv()
    c7 = send_lat(7, xg.at[far * C + c], far, sib)
    make_rows(far * C + c)
    c5.wait_recv()
    make_rows(down * C + 1 - c)
    c6.wait_recv()
    make_rows(up * C + 1 - c)
    c7.wait_recv()
    make_rows(far * C + 1 - c)

    lane = lax.broadcasted_iota(jnp.int32, (GRID_W, HEAD), 1)
    is_row = lane < HEAD // 2
    is_first = lax.rem(lane, HEAD // 2) < HEAD // 4

    def unit_rows(v, gain):
        return v * lax.rsqrt(jnp.mean(v * v, axis=-1, keepdims=True) + NORM_EPS) * gain

    def turned(v, gain, j):
        cos = jnp.where(is_row, cr[j : j + 1, :], cos_c[...])
        sin = jnp.where(is_row, sr[j : j + 1, :], sin_c[...])
        v = unit_rows(v, gain)
        other = jnp.where(is_first, pltpu.roll(v, HEAD - HEAD // 4, 1), pltpu.roll(v, HEAD // 4, 1))
        return (v * cos + other * sin).astype(jnp.bfloat16)

    qg, kg = q_gain[...], k_gain[...]
    blocks = GROUP_ROWS // GRID_W

    def at(d, col, s, lo, n):
        return keys.at[pl.ds(ORDER[(d, col, s)] * UNIT + lo, n)]

    def swap_kv():
        return remote(kvb, keys.at[pl.ds(0, UNIT)], s_send.at[0], s_recv.at[0], partner)

    def swap_q():
        return remote(qt, qb, s_send.at[1], s_recv.at[1], partner)

    def ring(direction, t, kind):
        col = "nbr" if kind == "nbr" else "own"
        lo, n = (H1, H2) if kind == "h2" else (0, H1)
        if kind == "h2" and t == 4:
            n = H2 // 2
            lo = lo if direction > 0 else lo + n
        dst = 4 if t == 4 else direction * t
        i = (0 if direction > 0 else 12) + (t - 1) * 3 + KINDS.index(kind)
        return remote(
            at(direction * (t - 1), col, 0, lo, n), at(dst, col, 0, lo, n), z_send.at[i], z_recv.at[i],
            z_up if direction > 0 else z_down,
        )

    def used(direction, t, kind):
        return t < 4 or kind == "h2" or (kind == "own") == (direction > 0)

    def cross(d):
        i = DS.index(d)
        return remote(at(d, "own", 0, H1, H2), at(d, "nbr", 0, H1, H2), x_send.at[i], x_recv.at[i], nbr)

    def cross_h1():
        return remote(at(0, "own", 0, 0, H1), at(0, "nbr", 0, 0, H1), x_send.at[8], x_recv.at[8], nbr)

    def share(d, col):
        i = DS.index(d) + (0 if col == "own" else 8)
        return remote(at(d, col, 0, 0, UNIT), at(d, col, 1, 0, UNIT), d_send.at[i], d_recv.at[i], sib)

    half = 2 * HEAD // 2

    def weight(i):
        who = [
            (ow_in, me, 0, 2 * half, y_up), (ow_in, me, 0, 2 * half, y_down), (ow_in, me, 0, 2 * half, sib),
            (None, down * C + c, 0, half, y_up), (None, up * C + c, half, half, y_down),
            (None, down * C + c, 0, 2 * half, sib), (None, up * C + c, 0, 2 * half, sib),
            (None, far * C + c, 0, 2 * half, sib),
        ][i]
        src, slot, lo, n, dev = who
        dst = ow.at[slot, pl.ds(lo, n)]
        return remote(dst if src is None else src, dst, o_send.at[i], o_recv.at[i], dev)

    def on_ring(t, kind):
        for direction in (1, -1):
            if used(direction, t, kind):
                ring(direction, t, kind).wait_recv()
            if t < 4 and used(direction, t + 1, kind):
                ring(direction, t + 1, kind).start()


    for i in range(3):
        weight(i).start()
    proj = jnp.dot(xn[...], wkv[...], preferred_element_type=jnp.float32)
    kvb[:CTX_ROWS, :HEAD] = unit_rows(proj[:CTX_ROWS, :HEAD], kg).astype(jnp.bfloat16)
    kvb[:CTX_ROWS, HEAD:] = proj[:CTX_ROWS, HEAD:].astype(jnp.bfloat16) * jnp.bfloat16(LIFT)
    for j in range(blocks):
        lo = CTX_ROWS + GRID_W * j
        kvb[lo : lo + GRID_W, :HEAD] = turned(proj[lo : lo + GRID_W, :HEAD], kg, j)
        kvb[lo : lo + GRID_W, HEAD:] = proj[lo : lo + GRID_W, HEAD:].astype(jnp.bfloat16)

    @pl.when(swapped)
    def _():
        swap_kv().start()

    @pl.when(jnp.logical_not(swapped))
    def _():
        keys[:UNIT, :] = kvb[...]

    def launch():
        cross_h1().start()
        for kind in ("own", "h2"):
            for direction in (1, -1):
                ring(direction, 1, kind).start()
        share(0, "own").start()
        cross(0).start()

    @pl.when(jnp.logical_not(swapped))
    def _():
        launch()

    proj = jnp.dot(xn[CTX_ROWS:, :], wqs[...], preferred_element_type=jnp.float32)
    for j in range(blocks):
        lo = GRID_W * j
        for h in range(2):
            qt[h * GROUP_ROWS + lo : h * GROUP_ROWS + lo + GRID_W, :] = turned(
                proj[lo : lo + GRID_W, h * HEAD : (h + 1) * HEAD], qg, j
            )

    @pl.when(swapped)
    def _():
        swap_q().start()
        swap_kv().wait_recv()
        launch()

    @pl.when(jnp.logical_not(swapped))
    def _():
        qb[...] = qt[...]

    def own_done(t):
        on_ring(t, "h2")
        for d in ((t, -t) if t < 4 else (4,)):
            cross(d).start()
            share(d, "own").start()

    def nbr_done(t):
        for d in ((t, -t) if 0 < t < 4 else (t,)):
            cross(d).wait_recv()
            share(d, "nbr").start()

    def shared(t, col):
        for d in ((t, -t) if 0 < t < 4 else (t,)):
            share(d, col).wait_recv()

    def step0():
        cross_h1().wait_recv()
        for direction in (1, -1):
            ring(direction, 1, "nbr").start()
        on_ring(1, "own")
        nbr_done(0)
        own_done(1)

        @pl.when(swapped)
        def _():
            swap_q().wait_recv()

        shared(0, "own")

    def step1():
        shared(0, "nbr")
        on_ring(1, "nbr")

    def step2():
        shared(1, "own")
        on_ring(2, "own")

    def step3():
        own_done(2)
        shared(2, "own")

    def step4():
        for i in (0, 1):
            weight(i).wait_recv()
        for i in (3, 4, 5, 6):
            weight(i).start()
        nbr_done(1)
        on_ring(2, "nbr")

    def step5():
        shared(1, "nbr")
        on_ring(3, "own")

    def step6():
        own_done(3)
        shared(3, "own")

    def step7():
        nbr_done(2)
        on_ring(3, "nbr")

    def step8():
        shared(2, "nbr")

    def step9():
        on_ring(4, "own")
        own_done(4)
        nbr_done(3)
        shared(4, "own")

    def step10():
        for i in (3, 4):
            weight(i).wait_recv()
        weight(7).start()
        shared(3, "nbr")

    def step11():
        on_ring(4, "nbr")
        nbr_done(4)
        shared(4, "nbr")

    steps = (step0, step1, step2, step3, step4, step5, step6, step7, step8, step9, step10, step11)


    def chunk(i, carry):
        for j, step in enumerate(steps):
            pl.when(i == j)(step)
        rows = pl.ds(pl.multiple_of(i * CHUNK, CHUNK), CHUNK)
        k = keys[rows, :HEAD]
        q = qb[...]
        scores = [
            lax.dot_general(k[a : a + SUB], q, (((1,), (1,)), ((), ())), preferred_element_type=jnp.float32)
            for a in range(0, CHUNK, SUB)
        ]
        weights = ones[:, pl.ds(pl.multiple_of(lax.rem(i, 3) * CHUNK, HEAD), CHUNK)]
        v = jnp.concatenate([keys[rows, HEAD:].T, weights], axis=0)
        m_old = m_ref[0:1, :]
        m_new = m_old
        for s in scores:
            m_new = jnp.maximum(m_new, jnp.max(s, axis=0, keepdims=True))
        p = jnp.concatenate([jnp.exp2((s - m_new) * SCORE_SCALE).astype(jnp.bfloat16) for s in scores], axis=0)
        fade = jnp.exp2((m_old - m_new) * SCORE_SCALE)
        acc[...] = acc[...] * fade + jnp.dot(v, p, preferred_element_type=jnp.float32)
        m_ref[...] = jnp.broadcast_to(m_new, m_ref.shape)
        return carry

    lax.fori_loop(0, CHUNKS, chunk, 0)

    for h in range(2):
        sl = pl.ds(h * GROUP_ROWS, GROUP_ROWS)
        att[:, h * HEAD : (h + 1) * HEAD] = (acc[:HEAD, sl] / acc[HEAD : HEAD + 1, sl]).T.astype(jnp.bfloat16)

    def hand(i):
        ry, rc = rel[i]
        yy, cc = lax.rem(y + ry, Y), c + rc * flip
        src = att.at[pl.ds(pl.multiple_of((yy * C + cc) * ROWS, ROWS), ROWS)]
        return remote(src, got.at[head], a_send.at[i], a_recv.at[head], (z, row_x, yy, cc))

    for i in range(1, Y * C):
        hand(i).start()

    @pl.when(swapped)
    def _():
        hand(0).start()

    @pl.when(jnp.logical_not(swapped))
    def _():
        got[head] = att[pl.ds(pl.multiple_of(me * ROWS, ROWS), ROWS), :]

    for i in (2, 5, 6, 7):
        weight(i).wait_recv()
    for j in range(Y * C):

        @pl.when(jnp.logical_or(swapped, head != j))
        def _():
            remote(att.at[pl.ds(0, ROWS)], got.at[j], a_send.at[0], a_recv.at[j], sib).wait_recv()

    rows = jnp.concatenate([got[j] for j in range(Y * C)], axis=1)
    for n in range(0, D, 512):
        total = jnp.zeros((ROWS, 512), jnp.float32)
        for j in range(Y * C):
            total = total + jnp.dot(
                rows[:, j * 2 * HEAD : (j + 1) * 2 * HEAD], ow[j, :, n : n + 512], preferred_element_type=jnp.float32
            )
        mixed[:, n : n + 512] = total
    v = mixed[...]
    v = v * lax.rsqrt(jnp.mean(v * v, axis=-1, keepdims=True) + NORM_EPS)
    out[...] = (lat[...].astype(jnp.float32) + mod_row(0, 32) * v).astype(jnp.bfloat16)

    for kind in KINDS:
        for t in range(1, 5):
            for direction in (1, -1):
                if used(direction, t, kind):
                    ring(direction, t, kind).wait_send()
    for d in DS:
        cross(d).wait_send()
        share(d, "own").wait_send()
        share(d, "nbr").wait_send()
    cross_h1().wait_send()
    for i in range(8):
        weight(i).wait_send()
    for i in range(1, Y * C):
        hand(i).wait_send()


    for s in lat_sends + xs + zs + ts:
        s.wait_send()

    @pl.when(swapped)
    def _():
        hand(0).wait_send()
        swap_kv().wait_send()
        swap_q().wait_send()


def layer(latents, context, cond, ctx_cond, mod_weight, wq, wk, wv, out_weight, q_gain, k_gain):
    hbm = pl.BlockSpec(memory_space=pltpu.HBM)
    bf, f32 = jnp.bfloat16, jnp.float32
    dma = pltpu.SemaphoreType.DMA
    return pl.pallas_call(
        layer_kernel,
        name="layer",
        out_shape=jax.ShapeDtypeStruct((ROWS, D), bf),
        in_specs=[hbm] * 15,
        out_specs=pl.BlockSpec(memory_space=pltpu.VMEM),
        scratch_shapes=[
            pltpu.VMEM((ROWS, D), bf),
            pltpu.VMEM((CTX_ROWS, D), bf),
            pltpu.VMEM((1, ROWS), f32),
            pltpu.VMEM((1, ROWS), f32),
            pltpu.VMEM((ROWS, 6 * HEAD), f32),
            pltpu.VMEM((1, HEAD), f32),
            pltpu.VMEM((1, HEAD), f32),
            pltpu.VMEM((GRID_W, HEAD), f32),
            pltpu.VMEM((GRID_W, HEAD), f32),
            pltpu.VMEM((8, HEAD), f32),
            pltpu.VMEM((8, HEAD), f32),
            pltpu.VMEM((Y * C, ROWS, D), bf),
            pltpu.VMEM((D, 2 * HEAD), bf),
            pltpu.VMEM((D, 2 * HEAD), bf),
            pltpu.VMEM((16, HEAD), f32),
            pltpu.VMEM((X - 1, 16, HEAD), f32),
            pltpu.VMEM((16, HEAD), f32),
            pltpu.VMEM((Z - 1, 16, HEAD), f32),
            pltpu.VMEM((Y * C, 16, HEAD), f32),
            pltpu.VMEM((UNIT, D), bf),
            pltpu.VMEM((UNIT, 2 * HEAD), bf),
            pltpu.VMEM((2 * GROUP_ROWS, HEAD), bf),
            pltpu.VMEM((TOTAL_KEYS, 2 * HEAD), bf),
            pltpu.VMEM((2 * GROUP_ROWS, HEAD), bf),
            pltpu.VMEM((16, 3 * CHUNK), bf),
            pltpu.VMEM((8, 2 * GROUP_ROWS), f32),
            pltpu.VMEM((HEAD + 16, 2 * GROUP_ROWS), f32),
            pltpu.VMEM((GROUP_ROWS, 2 * HEAD), bf),
            pltpu.VMEM((Y * C, ROWS, 2 * HEAD), bf),
            pltpu.VMEM((Y * C, 2 * HEAD, D), bf),
            pltpu.VMEM((ROWS, D), f32),
            dma((15,)), dma((8,)), dma((8,)), dma((3,)), dma((3,)), dma((7,)), dma((7,)), dma((7,)), dma((7,)),
            dma((24,)), dma((24,)), dma((9,)), dma((9,)), dma((16,)), dma((16,)),
            dma((8,)), dma((8,)), dma((2,)), dma((2,)), dma((8,)), dma((8,)),
        ],
        compiler_params=pltpu.CompilerParams(collective_id=0, has_side_effects=True, vmem_limit_bytes=62 << 20),
    )(
        latents, context, cond.reshape(1, -1), ctx_cond.reshape(1, -1), mod_weight, wq, wk, wv, out_weight,
        q_gain.reshape(1, -1), k_gain.reshape(1, -1), *rope_tables(),
    )


def solution(mesh):
    torus = Mesh(mesh.devices.reshape(Z, X, Y, C), AXES)
    placed = (
        P(AXES, None), P(SP, None), P(SP), P(SP), P(SP, TP), P(None, TP), P(None, TP), P(None, TP),
        P(TP, None), P(), P(),
    )
    return jax.shard_map(layer, mesh=torus, in_specs=placed, out_specs=P(AXES, None), check_vma=False)
```

time: 104 us -> 89.9 us (0.86)
  local copies, waits for them, and re-layouts: 13.7 us -> 1.67 us
  Pallas kernels: 89.7 us -> 88.1 us
    unnamed x35 -> x1, local copies, waits for them, and re-layouts: 13.7 us -> 1.67 us
    pallas_call x2 -> x1, Pallas kernels: 89.7 us -> 88.1 us  [layer(): pl.pallas_call(layer_kernel, name='layer', out_shape=jax.ShapeDtypeStruct...]
where the time goes in v3:
time: 89.9 us; the launch traced here: 89.8 us
  Pallas kernels  88.1 us (98%)
  local copies, waits for them, and re-layouts  1.67 us (2%)
    pallas_call x1, Pallas kernels, layer(): pl.pallas_call(layer_kernel, name='layer', out_shape=jax.ShapeDtypeStruct...  88.1 us

profile of v3, /device:TPU:1, one launch (start us, length us, event | category | flops | bytes accessed | tf_op | source)
XLA Modules:
  0.0 89.8 jit_solution(10273176542999700658)
XLA Ops:
  0.0 88.1 %layer.1 = bf16[64,2048]{1,0:T(8,128)(2,1)} custom-call(bf16[64,2048]{1,0:T(8,128)(2,1)} %lat_in.1, bf16[16,2048]{1,0:T(8,128)(2,1)} %ctx_in.1, f32[1,64]{1,0:T(1,128)} %bitcast.4, f32[1,64]{1,0:T(1,128)} %bitcast.5, f32[64,768]{1,0:T(8,128)} %modw_in.1, bf16[2048,256]{1,0:T(8,128)(2,1)} %wq.1, bf16[2048,128]{1,0:T(8,128)(2,1)} %wk.1, bf16[2048,128]{1,0:T(8,128)(2,1)} %wv.1, ...), custom_call_target="tpu_custom_call" | custom-call | tf_op jit(solution)/shard_map/layer/pallas_call | solution.py:525
  88.2 1.7 %copy.17 = bf16[64,2048]{1,0:T(8,128)(2,1)} copy(bf16[64,2048]{1,0:T(8,128)(2,1)} %layer.1) | data formatting | bytes 524288

commit v4 on v3

--- a/solution.py
+++ b/solution.py
@@ -78,7 +78,7 @@
 
 def unit_order():
     order = [(0, "own", s) for s in (0, 1)] + [(0, "nbr", s) for s in (0, 1)]
-    for t, col in ((1, "own"), (2, "own"), (1, "nbr"), (3, "own"), (2, "nbr"), (4, "own"), (3, "nbr"), (4, "nbr")):
+    for t, col in ((1, "own"), (1, "nbr"), (2, "own"), (2, "nbr"), (3, "own"), (3, "nbr"), (4, "own"), (4, "nbr")):
         for s in (0, 1):
             order += [(d, col, s) for d in ((t, -t) if t < 4 else (4,))]
     return {u: i for i, u in enumerate(order)}
@@ -139,9 +139,13 @@
         lat_sends.append(copy)
         return copy
 
-    c0 = send_lat(0, lat_in, y, y_up)
-    c1 = send_lat(1, lat_in, y, y_down)
-    c2 = send_lat(2, lat_in, y, sib)
+    hr = ROWS // 2
+    low, high = pl.ds(0, hr), pl.ds(hr, hr)
+    up_a = send_lat(0, lat_in.at[low], y, y_up, 0, hr)
+    down_a = send_lat(1, lat_in.at[high], y, y_down, hr, hr)
+    up_b = send_lat(2, lat_in.at[high], y, y_up, hr, hr)
+    down_b = send_lat(3, lat_in.at[low], y, y_down, 0, hr)
+    own = send_lat(4, lat_in, y, sib)
     for copy in loads[:5]:
         copy.wait()
 
@@ -169,13 +173,10 @@
     for s in zs:
         s.start()
 
-    hr = ROWS // 2
-    c0.wait_recv()
-    c3 = send_lat(3, xg.at[down * C + c, pl.ds(0, hr)], down, y_up, 0, hr)
-    c5 = send_lat(5, xg.at[down * C + c], down, sib)
-    c1.wait_recv()
-    c4 = send_lat(4, xg.at[up * C + c, pl.ds(hr, hr)], up, y_down, hr, hr)
-    c6 = send_lat(6, xg.at[up * C + c], up, sib)
+    up_a.wait_recv()
+    far_a = send_lat(5, xg.at[down * C + c, low], down, y_up, 0, hr)
+    down_a.wait_recv()
+    far_b = send_lat(6, xg.at[up * C + c, high], up, y_down, hr, hr)
 
     for s in zs:
         s.wait_recv()
@@ -186,8 +187,15 @@
     ts = [remote(mod.at[me], mod.at[me], mt_send.at[i], mt_recv.at[i], d) for i, d in enumerate(t_peers)]
     for s in ts:
         s.start()
+    up_b.wait_recv()
+    from_down = send_lat(7, xg.at[down * C + c], down, sib)
+    down_b.wait_recv()
+    from_up = send_lat(8, xg.at[up * C + c], up, sib)
     for copy in loads[5:]:
         copy.wait()
+    far_a.wait_recv()
+    far_b.wait_recv()
+    from_far = send_lat(9, xg.at[far * C + c], far, sib)
     for s in ts:
         s.wait_recv()
 
@@ -206,19 +214,16 @@
 
     xn[:CTX_ROWS, :] = modulated(ctx[...], 1)
     make_rows(me)
-    c2.wait_recv()
+    own.wait_recv()
     make_rows(y * C + 1 - c)
     make_rows(down * C + c)
     make_rows(up * C + c)
-    c3.wait_recv()
-    c4.wait_recv()
-    c7 = send_lat(7, xg.at[far * C + c], far, sib)
     make_rows(far * C + c)
-    c5.wait_recv()
+    from_down.wait_recv()
     make_rows(down * C + 1 - c)
-    c6.wait_recv()
+    from_up.wait_recv()
     make_rows(up * C + 1 - c)
-    c7.wait_recv()
+    from_far.wait_recv()
     make_rows(far * C + 1 - c)
 
     lane = lax.broadcasted_iota(jnp.int32, (GRID_W, HEAD), 1)
@@ -315,11 +320,11 @@
 
     def launch():
         cross_h1().start()
-        for kind in ("own", "h2"):
+        for kind in ("h2", "own"):
             for direction in (1, -1):
                 ring(direction, 1, kind).start()
+        cross(0).start()
         share(0, "own").start()
-        cross(0).start()
 
     @pl.when(jnp.logical_not(swapped))
     def _():
@@ -343,28 +348,35 @@
     def _():
         qb[...] = qt[...]
 
-    def own_done(t):
+    def both(t):
+        return (t, -t) if 0 < t < 4 else (t,)
+
+    def h2_in(t):
         on_ring(t, "h2")
-        for d in ((t, -t) if t < 4 else (4,)):
+        for d in both(t):
             cross(d).start()
+
+    def own_in(t):
+        on_ring(t, "own")
+        for d in both(t):
             share(d, "own").start()
 
-    def nbr_done(t):
-        for d in ((t, -t) if 0 < t < 4 else (t,)):
+    def nbr_in(t):
+        for d in both(t):
             cross(d).wait_recv()
             share(d, "nbr").start()
 
     def shared(t, col):
-        for d in ((t, -t) if 0 < t < 4 else (t,)):
+        for d in both(t):
             share(d, col).wait_recv()
 
-    def step0():
+    def before0():
         cross_h1().wait_recv()
         for direction in (1, -1):
             ring(direction, 1, "nbr").start()
-        on_ring(1, "own")
-        nbr_done(0)
-        own_done(1)
+        h2_in(1)
+        own_in(1)
+        nbr_in(0)
 
         @pl.when(swapped)
         def _():
@@ -372,63 +384,79 @@
 
         shared(0, "own")
 
-    def step1():
+    def before1():
         shared(0, "nbr")
         on_ring(1, "nbr")
 
-    def step2():
+    def before2():
         shared(1, "own")
-        on_ring(2, "own")
-
-    def step3():
-        own_done(2)
-        shared(2, "own")
-
-    def step4():
+
+    def within2():
+        h2_in(2)
+        nbr_in(1)
+
+    def before3():
+        shared(1, "nbr")
+
+    def within3():
+        own_in(2)
         for i in (0, 1):
             weight(i).wait_recv()
         for i in (3, 4, 5, 6):
             weight(i).start()
-        nbr_done(1)
+
+    def within4():
         on_ring(2, "nbr")
 
-    def step5():
-        shared(1, "nbr")
-        on_ring(3, "own")
-
-    def step6():
-        own_done(3)
+    def before5():
+        shared(2, "own")
+
+    def within5():
+        h2_in(3)
+        nbr_in(2)
+
+    def before6():
+        shared(2, "nbr")
+
+    def within6():
+        own_in(3)
+
+    def within7():
+        on_ring(3, "nbr")
+
+    def before8():
         shared(3, "own")
 
-    def step7():
-        nbr_done(2)
-        on_ring(3, "nbr")
-
-    def step8():
-        shared(2, "nbr")
-
-    def step9():
-        on_ring(4, "own")
-        own_done(4)
-        nbr_done(3)
+    def within8():
+        h2_in(4)
+        nbr_in(3)
+
+    def before9():
+        shared(3, "nbr")
+
+    def within9():
+        own_in(4)
+        on_ring(4, "nbr")
+
+    def before10():
         shared(4, "own")
 
-    def step10():
+    def within10():
+        nbr_in(4)
         for i in (3, 4):
             weight(i).wait_recv()
         weight(7).start()
-        shared(3, "nbr")
-
-    def step11():
-        on_ring(4, "nbr")
-        nbr_done(4)
+
+    def before11():
         shared(4, "nbr")
 
-    steps = (step0, step1, step2, step3, step4, step5, step6, step7, step8, step9, step10, step11)
-
+    before = {0: before0, 1: before1, 2: before2, 3: before3, 5: before5, 6: before6, 8: before8, 9: before9,
+              10: before10, 11: before11}
+    within = {2: within2, 3: within3, 4: within4, 5: within5, 6: within6, 7: within7, 8: within8, 9: within9,
+              10: within10}
 
     def chunk(i, carry):
-        for j, step in enumerate(steps):
+        for j, step in before.items():
             pl.when(i == j)(step)
         rows = pl.ds(pl.multiple_of(i * CHUNK, CHUNK), CHUNK)
         k = keys[rows, :HEAD]
@@ -443,6 +471,8 @@
         m_new = m_old
         for s in scores:
             m_new = jnp.maximum(m_new, jnp.max(s, axis=0, keepdims=True))
+        for j, step in within.items():
+            pl.when(i == j)(step)
         p = jnp.concatenate([jnp.exp2((s - m_new) * SCORE_SCALE).astype(jnp.bfloat16) for s in scores], axis=0)
         fade = jnp.exp2((m_old - m_new) * SCORE_SCALE)
         acc[...] = acc[...] * fade + jnp.dot(v, p, preferred_element_type=jnp.float32)
@@ -560,7 +590,7 @@
             pltpu.VMEM((Y * C, ROWS, 2 * HEAD), bf),
             pltpu.VMEM((Y * C, 2 * HEAD, D), bf),
             pltpu.VMEM((ROWS, D), f32),
-            dma((15,)), dma((8,)), dma((8,)), dma((3,)), dma((3,)), dma((7,)), dma((7,)), dma((7,)), dma((7,)),
+            dma((15,)), dma((10,)), dma((10,)), dma((3,)), dma((3,)), dma((7,)), dma((7,)), dma((7,)), dma((7,)),
             dma((24,)), dma((24,)), dma((9,)), dma((9,)), dma((16,)), dma((16,)),
             dma((8,)), dma((8,)), dma((2,)), dma((2,)), dma((8,)), dma((8,)),
         ],

time: 89.9 us -> 82.1 us (0.913)
  Pallas kernels: 88.1 us -> 80.3 us
    pallas_call x1, Pallas kernels: 88.1 us -> 80.3 us  [layer(): pl.pallas_call(layer_kernel, name='layer', out_shape=jax.ShapeDtypeStruct...]
where the time goes in v4:
time: 82.1 us; the launch traced here: 82 us
  Pallas kernels  80.3 us (98%)
  local copies, waits for them, and re-layouts  1.67 us (2%)
    pallas_call x1, Pallas kernels, layer(): pl.pallas_call(layer_kernel, name='layer', out_shape=jax.ShapeDtypeStruct...  80.3 us
    unnamed x1, local copies, waits for them, and re-layouts  1.67 us

profile of v4, /device:TPU:1, one launch (start us, length us, event | category | flops | bytes accessed | tf_op | source)
XLA Modules:
  0.0 82.0 jit_solution(10963836525985332319)
XLA Ops:
  0.0 80.3 %layer.1 = bf16[64,2048]{1,0:T(8,128)(2,1)} custom-call(bf16[64,2048]{1,0:T(8,128)(2,1)} %lat_in.1, bf16[16,2048]{1,0:T(8,128)(2,1)} %ctx_in.1, f32[1,64]{1,0:T(1,128)} %bitcast.4, f32[1,64]{1,0:T(1,128)} %bitcast.5, f32[64,768]{1,0:T(8,128)} %modw_in.1, bf16[2048,256]{1,0:T(8,128)(2,1)} %wq.1, bf16[2048,128]{1,0:T(8,128)(2,1)} %wk.1, bf16[2048,128]{1,0:T(8,128)(2,1)} %wv.1, ...), custom_call_target="tpu_custom_call" | custom-call | tf_op jit(solution)/shard_map/layer/pallas_call | solution.py:555
  80.3 1.7 %copy.17 = bf16[64,2048]{1,0:T(8,128)(2,1)} copy(bf16[64,2048]{1,0:T(8,128)(2,1)} %layer.1) | data formatting | bytes 524288

commit v5 on v4

--- a/solution.py
+++ b/solution.py
@@ -226,28 +226,32 @@
     from_far.wait_recv()
     make_rows(far * C + 1 - c)
 
-    lane = lax.broadcasted_iota(jnp.int32, (GRID_W, HEAD), 1)
+    piece = GRID_W // 2
+    lane = lax.broadcasted_iota(jnp.int32, (piece, HEAD), 1)
     is_row = lane < HEAD // 2
     is_first = lax.rem(lane, HEAD // 2) < HEAD // 4
 
     def unit_rows(v, gain):
         return v * lax.rsqrt(jnp.mean(v * v, axis=-1, keepdims=True) + NORM_EPS) * gain
 
-    def turned(v, gain, j):
-        cos = jnp.where(is_row, cr[j : j + 1, :], cos_c[...])
-        sin = jnp.where(is_row, sr[j : j + 1, :], sin_c[...])
+    def turned(v, gain, row):
+        j, o, n = row // GRID_W, row % GRID_W, v.shape[0]
+        cos = jnp.where(is_row, cr[j : j + 1, :], cos_c[o : o + n, :])
+        sin = jnp.where(is_row, sr[j : j + 1, :], sin_c[o : o + n, :])
         v = unit_rows(v, gain)
         other = jnp.where(is_first, pltpu.roll(v, HEAD - HEAD // 4, 1), pltpu.roll(v, HEAD // 4, 1))
         return (v * cos + other * sin).astype(jnp.bfloat16)
 
     qg, kg = q_gain[...], k_gain[...]
-    blocks = GROUP_ROWS // GRID_W
 
     def at(d, col, s, lo, n):
         return keys.at[pl.ds(ORDER[(d, col, s)] * UNIT + lo, n)]
 
-    def swap_kv():
-        return remote(kvb, keys.at[pl.ds(0, UNIT)], s_send.at[0], s_recv.at[0], partner)
+    parts = {"h1": pl.ds(0, H1), "h2": pl.ds(H1, H2)}
+
+    def swap_kv(part):
+        i = 0 if part == "h1" else 2
+        return remote(kvb.at[parts[part]], keys.at[parts[part]], s_send.at[i], s_recv.at[i], partner)
 
     def swap_q():
         return remote(qt, qb, s_send.at[1], s_recv.at[1], partner)
@@ -302,47 +306,51 @@
 
     for i in range(3):
         weight(i).start()
-    proj = jnp.dot(xn[...], wkv[...], preferred_element_type=jnp.float32)
-    kvb[:CTX_ROWS, :HEAD] = unit_rows(proj[:CTX_ROWS, :HEAD], kg).astype(jnp.bfloat16)
-    kvb[:CTX_ROWS, HEAD:] = proj[:CTX_ROWS, HEAD:].astype(jnp.bfloat16) * jnp.bfloat16(LIFT)
-    for j in range(blocks):
-        lo = CTX_ROWS + GRID_W * j
-        kvb[lo : lo + GRID_W, :HEAD] = turned(proj[lo : lo + GRID_W, :HEAD], kg, j)
-        kvb[lo : lo + GRID_W, HEAD:] = proj[lo : lo + GRID_W, HEAD:].astype(jnp.bfloat16)
-
-    @pl.when(swapped)
-    def _():
-        swap_kv().start()
-
-    @pl.when(jnp.logical_not(swapped))
-    def _():
-        keys[:UNIT, :] = kvb[...]
-
-    def launch():
-        cross_h1().start()
-        for kind in ("h2", "own"):
-            for direction in (1, -1):
-                ring(direction, 1, kind).start()
-        cross(0).start()
-        share(0, "own").start()
-
-    @pl.when(jnp.logical_not(swapped))
-    def _():
-        launch()
+
+    def make_kv(lo, hi):
+        proj = jnp.dot(xn[lo:hi, :], wkv[...], preferred_element_type=jnp.float32)
+        if lo == 0:
+            kvb[:CTX_ROWS, :HEAD] = unit_rows(proj[:CTX_ROWS, :HEAD], kg).astype(jnp.bfloat16)
+            kvb[:CTX_ROWS, HEAD:] = proj[:CTX_ROWS, HEAD:].astype(jnp.bfloat16) * jnp.bfloat16(LIFT)
+        for r in range(max(lo, CTX_ROWS), hi, piece):
+            rows = proj[r - lo : r - lo + piece]
+            kvb[r : r + piece, :HEAD] = turned(rows[:, :HEAD], kg, r - CTX_ROWS)
+            kvb[r : r + piece, HEAD:] = rows[:, HEAD:].astype(jnp.bfloat16)
+
+    def launch(part):
+        if part == "h1":
+            cross_h1().start()
+        for direction in (1, -1):
+            ring(direction, 1, "own" if part == "h1" else "h2").start()
+        if part == "h1":
+            cross(0).start()
+            share(0, "own").start()
+
+    for part, lo, hi in (("h2", H1, UNIT), ("h1", 0, H1)):
+        make_kv(lo, hi)
+
+        @pl.when(swapped)
+        def _():
+            swap_kv(part).start()
+
+        @pl.when(jnp.logical_not(swapped))
+        def _():
+            keys[lo:hi, :] = kvb[lo:hi, :]
+            launch(part)
 
     proj = jnp.dot(xn[CTX_ROWS:, :], wqs[...], preferred_element_type=jnp.float32)
-    for j in range(blocks):
-        lo = GRID_W * j
+    for r in range(0, GROUP_ROWS, piece):
         for h in range(2):
-            qt[h * GROUP_ROWS + lo : h * GROUP_ROWS + lo + GRID_W, :] = turned(
-                proj[lo : lo + GRID_W, h * HEAD : (h + 1) * HEAD], qg, j
+            qt[h * GROUP_ROWS + r : h * GROUP_ROWS + r + piece, :] = turned(
+                proj[r : r + piece, h * HEAD : (h + 1) * HEAD], qg, r
             )
 
     @pl.when(swapped)
     def _():
         swap_q().start()
-        swap_kv().wait_recv()
-        launch()
+        for part in ("h2", "h1"):
+            swap_kv(part).wait_recv()
+            launch(part)
 
     @pl.when(jnp.logical_not(swapped))
     def _():
@@ -386,6 +394,8 @@
 
     def before1():
         shared(0, "nbr")
+
+    def within1():
         on_ring(1, "nbr")
 
     def before2():
@@ -400,13 +410,13 @@
 
     def within3():
         own_in(2)
+
+    def within4():
+        on_ring(2, "nbr")
         for i in (0, 1):
             weight(i).wait_recv()
         for i in (3, 4, 5, 6):
             weight(i).start()
-
-    def within4():
-        on_ring(2, "nbr")
 
     def before5():
         shared(2, "own")
@@ -451,56 +461,66 @@
         shared(4, "nbr")
 
     before = {0: before0, 1: before1, 2: before2, 3: before3, 5: before5, 6: before6, 8: before8, 9: before9,
-              10: before10, 11: before11}
-    within = {2: within2, 3: within3, 4: within4, 5: within5, 6: within6, 7: within7, 8: within8, 9: within9,
+              10: before10}
+    within = {1: within1, 2: within2, 3: within3, 4: within4, 5: within5, 6: within6, 7: within7, 8: within8, 9: within9,
               10: within10}
 
-    def chunk(i, carry):
-        for j, step in before.items():
-            pl.when(i == j)(step)
+    def flash(i, sl, between):
         rows = pl.ds(pl.multiple_of(i * CHUNK, CHUNK), CHUNK)
         k = keys[rows, :HEAD]
-        q = qb[...]
+        q = qb[sl, :]
         scores = [
             lax.dot_general(k[a : a + SUB], q, (((1,), (1,)), ((), ())), preferred_element_type=jnp.float32)
             for a in range(0, CHUNK, SUB)
         ]
         weights = ones[:, pl.ds(pl.multiple_of(lax.rem(i, 3) * CHUNK, HEAD), CHUNK)]
         v = jnp.concatenate([keys[rows, HEAD:].T, weights], axis=0)
-        m_old = m_ref[0:1, :]
+        m_old = m_ref[0:1, sl]
         m_new = m_old
         for s in scores:
             m_new = jnp.maximum(m_new, jnp.max(s, axis=0, keepdims=True))
-        for j, step in within.items():
-            pl.when(i == j)(step)
+        between()
         p = jnp.concatenate([jnp.exp2((s - m_new) * SCORE_SCALE).astype(jnp.bfloat16) for s in scores], axis=0)
         fade = jnp.exp2((m_old - m_new) * SCORE_SCALE)
-        acc[...] = acc[...] * fade + jnp.dot(v, p, preferred_element_type=jnp.float32)
+        total = acc[:, sl] * fade + jnp.dot(v, p, preferred_element_type=jnp.float32)
+        return total, m_new
+
+    def chunk(i, carry):
+        for j, step in before.items():
+            pl.when(i == j)(step)
+
+        def between():
+            for j, step in within.items():
+                pl.when(i == j)(step)
+
+        total, m_new = flash(i, pl.ds(0, 2 * GROUP_ROWS), between)
+        acc[...] = total
         m_ref[...] = jnp.broadcast_to(m_new, m_ref.shape)
         return carry
 
-    lax.fori_loop(0, CHUNKS, chunk, 0)
-
-    for h in range(2):
-        sl = pl.ds(h * GROUP_ROWS, GROUP_ROWS)
-        att[:, h * HEAD : (h + 1) * HEAD] = (acc[:HEAD, sl] / acc[HEAD : HEAD + 1, sl]).T.astype(jnp.bfloat16)
-
-    def hand(i):
+    lax.fori_loop(0, CHUNKS - 1, chunk, 0)
+    before11()
+
+    def hand(i, h):
         ry, rc = rel[i]
         yy, cc = lax.rem(y + ry, Y), c + rc * flip
-        src = att.at[pl.ds(pl.multiple_of((yy * C + cc) * ROWS, ROWS), ROWS)]
-        return remote(src, got.at[head], a_send.at[i], a_recv.at[head], (z, row_x, yy, cc))
-
-    for i in range(1, Y * C):
-        hand(i).start()
-
-    @pl.when(swapped)
-    def _():
-        hand(0).start()
-
-    @pl.when(jnp.logical_not(swapped))
-    def _():
-        got[head] = att[pl.ds(pl.multiple_of(me * ROWS, ROWS), ROWS), :]
+        src = att.at[h, pl.ds(pl.multiple_of((yy * C + cc) * ROWS, ROWS), ROWS)]
+        return remote(src, got.at[h, head], a_send.at[h, i], a_recv.at[h, head], (z, row_x, yy, cc))
+
+    far_first = sorted(range(1, Y * C), key=lambda i: -min(rel[i][0], Y - rel[i][0]))
+    for h in range(2):
+        total, _ = flash(CHUNKS - 1, pl.ds(h * GROUP_ROWS, GROUP_ROWS), lambda: None)
+        att[h] = (total[:HEAD] / total[HEAD : HEAD + 1]).T.astype(jnp.bfloat16)
+        for i in far_first:
+            hand(i, h).start()
+
+        @pl.when(swapped)
+        def _():
+            hand(0, h).start()
+
+        @pl.when(jnp.logical_not(swapped))
+        def _():
+            got[h, head] = att[h, pl.ds(pl.multiple_of(me * ROWS, ROWS), ROWS), :]
 
     for i in (2, 5, 6, 7):
         weight(i).wait_recv()
@@ -508,9 +528,10 @@
 
         @pl.when(jnp.logical_or(swapped, head != j))
         def _():
-            remote(att.at[pl.ds(0, ROWS)], got.at[j], a_send.at[0], a_recv.at[j], sib).wait_recv()
-
-    rows = jnp.concatenate([got[j] for j in range(Y * C)], axis=1)
+            for h in range(2):
+                remote(att.at[h, pl.ds(0, ROWS)], got.at[h, j], a_send.at[h, 0], a_recv.at[h, j], sib).wait_recv()
+
+    rows = jnp.concatenate([got[h, j] for j in range(Y * C) for h in range(2)], axis=1)
     for n in range(0, D, 512):
         total = jnp.zeros((ROWS, 512), jnp.float32)
         for j in range(Y * C):
@@ -535,7 +556,8 @@
     for i in range(8):
         weight(i).wait_send()
     for i in range(1, Y * C):
-        hand(i).wait_send()
+        hand(i, 0).wait_send()
+        hand(i, 1).wait_send()
 
 
     for s in lat_sends + xs + zs + ts:
@@ -543,8 +565,10 @@
 
     @pl.when(swapped)
     def _():
-        hand(0).wait_send()
-        swap_kv().wait_send()
+        hand(0, 0).wait_send()
+        hand(0, 1).wait_send()
+        swap_kv("h1").wait_send()
+        swap_kv("h2").wait_send()
         swap_q().wait_send()
 
 
@@ -586,13 +610,13 @@
             pltpu.VMEM((16, 3 * CHUNK), bf),
             pltpu.VMEM((8, 2 * GROUP_ROWS), f32),
             pltpu.VMEM((HEAD + 16, 2 * GROUP_ROWS), f32),
-            pltpu.VMEM((GROUP_ROWS, 2 * HEAD), bf),
-            pltpu.VMEM((Y * C, ROWS, 2 * HEAD), bf),
+            pltpu.VMEM((2, GROUP_ROWS, HEAD), bf),
+            pltpu.VMEM((2, Y * C, ROWS, HEAD), bf),
             pltpu.VMEM((Y * C, 2 * HEAD, D), bf),
             pltpu.VMEM((ROWS, D), f32),
             dma((15,)), dma((10,)), dma((10,)), dma((3,)), dma((3,)), dma((7,)), dma((7,)), dma((7,)), dma((7,)),
             dma((24,)), dma((24,)), dma((9,)), dma((9,)), dma((16,)), dma((16,)),
-            dma((8,)), dma((8,)), dma((2,)), dma((2,)), dma((8,)), dma((8,)),
+            dma((8,)), dma((8,)), dma((3,)), dma((3,)), dma((2, 8)), dma((2, 8)),
         ],
         compiler_params=pltpu.CompilerParams(collective_id=0, has_side_effects=True, vmem_limit_bytes=62 << 20),
     )(

time: 82.1 us -> 79.1 us (0.963)
  Pallas kernels: 80.3 us -> 77.3 us
    pallas_call x1, Pallas kernels: 80.3 us -> 77.3 us  [layer(): pl.pallas_call(layer_kernel, name='layer', out_shape=jax.ShapeDtypeStruct...]
where the time goes in v5:
time: 79.1 us; the launch traced here: 79 us
  Pallas kernels  77.3 us (98%)
  local copies, waits for them, and re-layouts  1.67 us (2%)
    pallas_call x1, Pallas kernels, layer(): pl.pallas_call(layer_kernel, name='layer', out_shape=jax.ShapeDtypeStruct...  77.3 us
    unnamed x1, local copies, waits for them, and re-layouts  1.67 us

profile of v5, /device:TPU:1, one launch (start us, length us, event | category | flops | bytes accessed | tf_op | source)
XLA Modules:
  0.0 79.0 jit_solution(6269153015353944141)
XLA Ops:
  0.0 77.3 %layer.1 = bf16[64,2048]{1,0:T(8,128)(2,1)} custom-call(bf16[64,2048]{1,0:T(8,128)(2,1)} %lat_in.1, bf16[16,2048]{1,0:T(8,128)(2,1)} %ctx_in.1, f32[1,64]{1,0:T(1,128)} %bitcast.4, f32[1,64]{1,0:T(1,128)} %bitcast.5, f32[64,768]{1,0:T(8,128)} %modw_in.1, bf16[2048,256]{1,0:T(8,128)(2,1)} %wq.1, bf16[2048,128]{1,0:T(8,128)(2,1)} %wk.1, bf16[2048,128]{1,0:T(8,128)(2,1)} %wv.1, ...), custom_call_target="tpu_custom_call" | custom-call | tf_op jit(solution)/shard_map/layer/pallas_call | solution.py:579
  77.3 1.7 %copy.17 = bf16[64,2048]{1,0:T(8,128)(2,1)} copy(bf16[64,2048]{1,0:T(8,128)(2,1)} %layer.1) | data formatting | bytes 524288

commit v6 on v5

--- a/solution.py
+++ b/solution.py
@@ -244,7 +244,12 @@
 
     qg, kg = q_gain[...], k_gain[...]
 
+    late = 1 - lax.rem(is_a + c, 2)
+
     def at(d, col, s, lo, n):
+        if d == 0 and col == "nbr":
+            place = 2 + (1 - late if s else late)
+            return keys.at[pl.ds(pl.multiple_of(place * UNIT + lo, CTX_ROWS), n)]
         return keys.at[pl.ds(ORDER[(d, col, s)] * UNIT + lo, n)]
 
     parts = {"h1": pl.ds(0, H1), "h2": pl.ds(H1, H2)}
@@ -281,7 +286,8 @@
 
     def share(d, col):
         i = DS.index(d) + (0 if col == "own" else 8)
-        return remote(at(d, col, 0, 0, UNIT), at(d, col, 1, 0, UNIT), d_send.at[i], d_recv.at[i], sib)
+        there = 0 if d == 0 and col == "nbr" else 1
+        return remote(at(d, col, 0, 0, UNIT), at(d, col, there, 0, UNIT), d_send.at[i], d_recv.at[i], sib)
 
     half = 2 * HEAD // 2
 
@@ -382,18 +388,31 @@
         cross_h1().wait_recv()
         for direction in (1, -1):
             ring(direction, 1, "nbr").start()
-        h2_in(1)
-        own_in(1)
-        nbr_in(0)
+
+        @pl.when(jnp.logical_not(swapped))
+        def _():
+            h2_in(1)
+            own_in(1)
+            nbr_in(0)
 
         @pl.when(swapped)
         def _():
             swap_q().wait_recv()
+            shared(0, "nbr")
 
         shared(0, "own")
 
+    def within0():
+        @pl.when(swapped)
+        def _():
+            h2_in(1)
+            own_in(1)
+            nbr_in(0)
+
     def before1():
-        shared(0, "nbr")
+        @pl.when(jnp.logical_not(swapped))
+        def _():
+            shared(0, "nbr")
 
     def within1():
         on_ring(1, "nbr")
@@ -462,7 +481,7 @@
 
     before = {0: before0, 1: before1, 2: before2, 3: before3, 5: before5, 6: before6, 8: before8, 9: before9,
               10: before10}
-    within = {1: within1, 2: within2, 3: within3, 4: within4, 5: within5, 6: within6, 7: within7, 8: within8, 9: within9,
+    within = {0: within0, 1: within1, 2: within2, 3: within3, 4: within4, 5: within5, 6: within6, 7: within7, 8: within8, 9: within9,
               10: within10}
 
     def flash(i, sl, between):

time: 79.1 us -> 79 us (level)
  no operation moved by 1% of the time
where the time goes in v6:
time: 79 us; the launch traced here: 78.9 us
  Pallas kernels  77.2 us (98%)
  local copies, waits for them, and re-layouts  1.67 us (2%)
    pallas_call x1, Pallas kernels, layer(): pl.pallas_call(layer_kernel, name='layer', out_shape=jax.ShapeDtypeStruct...  77.2 us
    unnamed x1, local copies, waits for them, and re-layouts  1.67 us

profile of v6, /device:TPU:1, one launch (start us, length us, event | category | flops | bytes accessed | tf_op | source)
XLA Modules:
  0.0 78.9 jit_solution(17883164347975469436)
XLA Ops:
  0.0 77.2 %layer.1 = bf16[64,2048]{1,0:T(8,128)(2,1)} custom-call(bf16[64,2048]{1,0:T(8,128)(2,1)} %lat_in.1, bf16[16,2048]{1,0:T(8,128)(2,1)} %ctx_in.1, f32[1,64]{1,0:T(1,128)} %bitcast.4, f32[1,64]{1,0:T(1,128)} %bitcast.5, f32[64,768]{1,0:T(8,128)} %modw_in.1, bf16[2048,256]{1,0:T(8,128)(2,1)} %wq.1, bf16[2048,128]{1,0:T(8,128)(2,1)} %wk.1, bf16[2048,128]{1,0:T(8,128)(2,1)} %wv.1, ...), custom_call_target="tpu_custom_call" | custom-call | tf_op jit(solution)/shard_map/layer/pallas_call | solution.py:598
  77.2 1.7 %copy.17 = bf16[64,2048]{1,0:T(8,128)(2,1)} copy(bf16[64,2048]{1,0:T(8,128)(2,1)} %layer.1) | data formatting | bytes 524288
